TPU v7x, 512 devices: a whole 4x4x16 slice. The times are simulated.
512 devices in a mesh: sp: 64 (over z, y), tp: 8 (over x, core).
Axes of the slice: x: 4, y: 4, z: 16, core: 2. Of those that a mesh axis runs over, the one named last changes fastest.
Arguments:
- queries: bfloat16 [8192, 768], P('sp', 'tp'), may hold values from -6 to 6
- latents: bfloat16 [8192, 512], P('sp'), may hold values from -6 to 6
- rot_key: bfloat16 [8192, 32], P('sp'), may hold values from -6 to 6
- kv_weight: bfloat16 [512, 1024], P(None, 'tp'), may hold values from -0.25 to 0.25
- log_sums: float32 [8192, 8], P('sp', 'tp'), may hold values from 4 to 14, as said below
- outputs: bfloat16 [8192, 512], P('sp', 'tp'), may hold values from -4 to 4
- out_grad: bfloat16 [8192, 512], P('sp', 'tp'), may hold values from -384 to 384
Outputs:
- query_grad: bfloat16 [8192, 768], P('sp', 'tp')
- key_grad: bfloat16 [8192, 512], P('sp', 'tp')
- value_grad: bfloat16 [8192, 512], P('sp', 'tp')
- rot_grad: float32 [8192, 32], P('sp')
- weight_grad: float32 [512, 1024], P('sp', 'tp')
Inputs may be any that keep to these rules, and one draw needn't show every extreme that they name: `log_sums`: each value lies within one half of log(8192) + 0.5.
All inputs are finite; a program needn't handle non-finite values.
Results may differ from a plain program's by a relative error of at most 0.004.
The roundings to bfloat16 on the way count: a program that leaves them out, or rounds other values in their place, can miss the bound.
Values may be sent and summed in bfloat16 or wider, within the bound.
No kernel may reach another device: no remote copies, remote signals or barrier semaphores. Data moves between devices by JAX's collectives and lax.ppermute only.
A program may use at most 64 MiB of HBM per device.

v0:
```python
import jax
import jax.numpy as jnp
from jax import lax
from jax.sharding import PartitionSpec as P

NOPE_DIM = 64
ROPE_DIM = 32
VALUE_DIM = 64


def in_one_piece(arrays, axis, dim, along):
    both = jnp.concatenate(arrays, axis=along)
    filled, at, outs = (lax.all_gather(both, axis, axis=dim, tiled=True), 0, [])
    for a in arrays:
        outs.append(lax.slice_in_dim(filled, at, at + a.shape[along], axis=along))
        at += a.shape[along]
    return tuple(outs)


def from_everyone(x, axis):
    copies = jnp.broadcast_to(x, (lax.axis_size(axis), *x.shape))
    return lax.all_to_all(copies, axis, split_axis=0, concat_axis=0, tiled=True)


def over_copies(x, axis):
    return from_everyone(x, axis).sum(axis=0)


def split_up(x, dim, length):
    before, after = (x.shape[:dim], x.shape[dim + 1 :])
    return jnp.moveaxis(x.reshape(*before, length, -1, *after), dim, 0)


def sent_and_summed(x, axis, dim):
    tiles = split_up(x, dim, lax.axis_size(axis))
    arrived = lax.all_to_all(tiles, axis, split_axis=0, concat_axis=0, tiled=True)
    return arrived.sum(axis=0)


def head_keys(joined_piece, rot_piece, head_count):
    piece_rows = joined_piece.shape[0]
    joined = joined_piece.reshape(piece_rows, head_count, NOPE_DIM + VALUE_DIM)
    rotary = rot_piece[:, None, :]
    return (jnp.concatenate([joined[:, :, :NOPE_DIM], rotary], axis=-1), joined[:, :, NOPE_DIM:])


def grad_scores(query_part, grad_part, key_full, values, log_part, delta_part):
    score_scale = (NOPE_DIM + ROPE_DIM) ** (-0.5)
    scores = (
        jnp.einsum("qhd,khd->hqk", query_part, key_full, preferred_element_type=jnp.float32)
        * score_scale
    )
    probs = jnp.exp(scores - log_part.T[:, :, None])
    dprob = jnp.einsum("qhd,khd->hqk", grad_part, values, preferred_element_type=jnp.float32)
    dscore = (probs * (dprob - delta_part.T[:, :, None])).astype(jnp.bfloat16)
    return (probs.astype(jnp.bfloat16), dscore)


def over_blocks(block_step, totals, pieces):
    piece_rows = pieces[0].shape[0]
    block_count = piece_rows // 1024
    stacked = tuple((member.reshape((block_count, 1024) + member.shape[1:]) for member in pieces))

    def scan_step(acc, item):
        block_index, parts = item
        return (block_step(acc, parts, block_index * 1024), None)

    totals, _ = lax.scan(scan_step, totals, (jnp.arange(block_count, dtype=jnp.int32), stacked))
    return totals


def per_device(queries, latents, rot_key, kv_weight, log_sums, outputs, out_grad):
    local_rows = queries.shape[0]
    head_count = log_sums.shape[1]
    head_dim = NOPE_DIM + ROPE_DIM
    score_scale = head_dim ** (-0.5)
    joined = jnp.dot(latents, kv_weight, preferred_element_type=jnp.float32).astype(jnp.bfloat16)
    own_keys, own_values = head_keys(joined, rot_key, head_count)
    own_queries = queries.reshape(local_rows, head_count, head_dim)
    own_grads = out_grad.reshape(local_rows, head_count, VALUE_DIM)
    row_delta = jnp.sum(
        outputs.astype(jnp.float32).reshape(local_rows, head_count, VALUE_DIM)
        * own_grads.astype(jnp.float32),
        axis=-1,
    )
    query_zero = jnp.zeros((local_rows, head_count, head_dim), jnp.float32)
    key_zero = jnp.zeros((local_rows, head_count, head_dim), jnp.float32)
    value_zero = jnp.zeros((local_rows, head_count, VALUE_DIM), jnp.float32)

    def query_step(query_total, pieces, start_row):
        keys_piece, values_piece = head_keys(pieces[0], pieces[1], head_count)
        probs_b, dscore = grad_scores(
            own_queries, own_grads, keys_piece, values_piece, log_sums, row_delta
        )
        return (
            query_total
            + jnp.einsum("hqk,khd->qhd", dscore, keys_piece, preferred_element_type=jnp.float32)
            * score_scale
        )

    query_total = over_blocks(query_step, query_zero, in_one_piece((joined, rot_key), "sp", 0, 1))
    all_logs, all_delta = in_one_piece((log_sums, row_delta), "sp", 0, 1)

    def key_step(totals, pieces, start_row):
        piece_rows = pieces[0].shape[0]
        query_part = pieces[0].reshape(piece_rows, head_count, head_dim)
        grad_part = pieces[1].reshape(piece_rows, head_count, VALUE_DIM)
        log_part = lax.dynamic_slice_in_dim(all_logs, start_row, piece_rows, 0)
        delta_part = lax.dynamic_slice_in_dim(all_delta, start_row, piece_rows, 0)
        probs_b, dscore = grad_scores(
            query_part, grad_part, own_keys, own_values, log_part, delta_part
        )
        key_next = (
            totals[0]
            + jnp.einsum("hqk,qhd->khd", dscore, query_part, preferred_element_type=jnp.float32)
            * score_scale
        )
        value_next = totals[1] + jnp.einsum(
            "hqk,qhd->khd", probs_b, grad_part, preferred_element_type=jnp.float32
        )
        return (key_next, value_next)

    key_total, value_total = over_blocks(
        key_step, (key_zero, value_zero), in_one_piece((queries, out_grad), "sp", 0, 1)
    )
    rot_grad = over_copies(jnp.sum(key_total[:, :, NOPE_DIM:], axis=1), "tp")
    key_grad = key_total[:, :, :NOPE_DIM].astype(jnp.bfloat16)
    value_grad = value_total.astype(jnp.bfloat16)
    stacked = jnp.concatenate([key_grad, value_grad], axis=-1).reshape(
        local_rows, head_count * (NOPE_DIM + VALUE_DIM)
    )
    weight_grad = sent_and_summed(
        lax.dot_general(
            latents, stacked, (((0,), (0,)), ((), ())), preferred_element_type=jnp.float32
        ),
        "sp",
        0,
    )
    query_grad = query_total.astype(jnp.bfloat16).reshape(local_rows, head_count * head_dim)
    return (
        query_grad,
        key_grad.reshape(local_rows, head_count * NOPE_DIM),
        value_grad.reshape(local_rows, head_count * VALUE_DIM),
        rot_grad,
        weight_grad,
    )


def solution(mesh):
    placed = (
        P("sp", "tp"),
        P("sp", None),
        P("sp", None),
        P(None, "tp"),
        P("sp", "tp"),
        P("sp", "tp"),
        P("sp", "tp"),
    )
    return jax.shard_map(
        per_device,
        mesh=mesh,
        in_specs=placed,
        out_specs=(P("sp", "tp"), P("sp", "tp"), P("sp", "tp"), P("sp", None), P("sp", "tp")),
        check_vma=False,
    )
```

profile of v0, /device:TPU:6, one launch (start us, length us, event | category | flops | bytes accessed | tf_op | source)
XLA Modules:
  0.0 337.4 jit_solution(9991707621675473649)
XLA Ops:
  7.2 1.4 pad_maximum_fusion.1
  8.7 1.1 convolution_convert_fusion
  9.8 1.3 pad_maximum_fusion
  12.6 88.7 %all_gather.11 = f32[8192,2]{0,1:T(2,128)S(1)} all-gather(f32[128,2]{0,1:T(2,128)S(1)} %pad_maximum_fusion.3), channel_id=1, replica_groups=mesh['sp'=64,'tp'=8] {'sp'}, dimensions={0}, use_global_device_ids=true | all-gather | bytes 66560 | tf_op jit(solution)/shard_map/all_gather | solution.py:13
  102.1 50.6 %all-gather.5.cloned.1.call-done = bf16[8192,160]{0,1:T(8,128)(2,1)} async-done(((bf16[128,160]{0,1:T(8,128)(2,1)}), bf16[8192,160]{0,1:T(8,128)(2,1)}) %all-gather.5.cloned.1.call-update) | async-done | bytes 2621456 | tf_op jit(solution)/shard_map/all_gather | solution.py:13
  152.7 2.7 slice.53
  155.4 3.2 copy.29
  158.6 1.8 copy.30
  160.4 33.0 %while.25 = (s32[]{:T(128)}, f32[128,1,96]{0,2,1:T(8,128)S(1)}, f32[128,1,64]{0,2,1:T(8,128)S(1)}, bf16[8,1024,96]{2,1,0:T(8,128)(2,1)S(1)}, bf16[128,1,96]{0,2,...) while((s32[]{:T(128)}, f32[128,1,96]{0,2,1:T(8,128)S(1)}, ...), condition=%wide.region_4.5_spmd.clone, body=%wide.region_3.4_spmd.clone.sunk | while | flops 84725760 | bytes 2852562 | solution.py:68
  161.9 1.4 fusion.80
  163.3 1.2 fusion.81
  166.0 1.4 fusion.80
  167.4 1.2 fusion.81
  170.1 1.4 fusion.80
  171.5 1.2 fusion.81
  174.2 1.4 fusion.80
  175.6 1.2 fusion.81
  178.4 1.4 fusion.80
  179.8 1.2 fusion.81
  182.5 1.4 fusion.80
  183.9 1.2 fusion.81
  186.6 1.4 fusion.80
  188.0 1.2 fusion.81
  190.7 1.4 fusion.80
  192.1 1.2 fusion.81
  194.0 4.8 %all-to-all-start = ((f32[8,128,32]{1,2,0:T(8,128)}), f32[8,128,32]{1,2,0:T(8,128)S(1)}, u32[]{:S(2)}, u32[]{:S(2)}) async-start(f32[8,128,32]{1,2,0:T(8,128)} %broadcast_in_dim.14), calls=%async_computation | async-start | bytes 262144 | tf_op jit(solution)/shard_map/all_to_all | solution.py:22
  199.8 89.0 %all-gather.3.cloned.1.call-done = bf16[8192,160]{0,1:T(8,128)(2,1)} async-done(((bf16[128,160]{0,1:T(8,128)(2,1)}), bf16[8192,160]{0,1:T(8,128)(2,1)}) %all-gather.3.cloned.1.call-update) | async-done | bytes 2621456 | tf_op jit(solution)/shard_map/all_gather | solution.py:13
  288.9 1.6 slice-done
  290.5 2.4 copy.32
  292.9 1.7 copy.33
  294.6 10.2 %all-to-all-start.1 = ((f32[64,8,128]{2,1,0:T(8,128)}), f32[64,8,128]{2,1,0:T(8,128)S(1)}, u32[]{:S(2)}, u32[]{:S(2)}) async-start(f32[64,8,128]{2,1,0:T(8,128)} %bitcast.15), calls=%async_computation.1 | async-start | bytes 524288 | tf_op jit(solution)/shard_map/all_to_all | solution.py:36
  304.9 22.6 %while.24 = (s32[]{:T(128)}, f32[128,1,96]{0,2,1:T(8,128)S(1)}, bf16[8,1024,128]{2,1,0:T(8,128)(2,1)}, bf16[8,1024,32]{2,1,0:T(8,128)(2,1)}, bf16[128,1,96]{0,2,...) while((s32[]{:T(128)}, f32[128,1,96]{0,2,1:T(8,128)S(1)}, ...), condition=%wide.region_2.3_spmd.clone, body=%wide.region_1.2_spmd.clone.sunk | while | flops 68587520 | bytes 2303095 | solution.py:68
  304.9 1.0 dynamic-slice_bitcast_fusion.4
  306.2 1.0 dynamic-slice_bitcast_fusion.5
  307.7 1.0 dynamic-slice_bitcast_fusion.4
  309.0 1.0 dynamic-slice_bitcast_fusion.5
  310.5 1.0 dynamic-slice_bitcast_fusion.4
  311.8 1.0 dynamic-slice_bitcast_fusion.5
  313.4 1.0 dynamic-slice_bitcast_fusion.4
  314.6 1.0 dynamic-slice_bitcast_fusion.5
  316.2 1.0 dynamic-slice_bitcast_fusion.4
  317.4 1.0 dynamic-slice_bitcast_fusion.5
  319.0 1.0 dynamic-slice_bitcast_fusion.4
  320.3 1.0 dynamic-slice_bitcast_fusion.5
  321.8 1.0 dynamic-slice_bitcast_fusion.4
  323.1 1.0 dynamic-slice_bitcast_fusion.5
  324.6 1.0 dynamic-slice_bitcast_fusion.4
  325.9 1.0 dynamic-slice_bitcast_fusion.5
  (79 shorter events, 20.5 us)
Async XLA Ops:
  7.2 1.5 copy-start
  7.2 145.5 %all-gather.5.cloned.1.call-start = ((), (), s32[]{:S(2)}) async-start(), calls=%async_computation.3 | async-start | bytes 2662400 | tf_op jit(solution)/shard_map/all_gather | solution.py:13
  8.7 280.2 %all-gather.3.cloned.1.call-start = ((), (), s32[]{:S(2)}) async-start(), calls=%async_computation.2 | async-start | bytes 2662400 | tf_op jit(solution)/shard_map/all_gather | solution.py:13
  155.4 3.2 slice-start.2
  194.0 100.6 %all-to-all-start = ((f32[8,128,32]{1,2,0:T(8,128)}), f32[8,128,32]{1,2,0:T(8,128)S(1)}, u32[]{:S(2)}, u32[]{:S(2)}) async-start(f32[8,128,32]{1,2,0:T(8,128)} %broadcast_in_dim.14), calls=%async_computation | async-start | bytes 262144 | tf_op jit(solution)/shard_map/all_to_all | solution.py:22
  288.9 1.6 slice-start
  290.4 2.4 slice-start.1
  292.9 12.0 %copy-start.1 = (bf16[128,96]{0,1:T(8,128)(2,1)S(1)}, bf16[128,96]{0,1:T(8,128)(2,1)}, u32[]{:S(2)}) copy-start(bf16[128,96]{0,1:T(8,128)(2,1)} %param.11) | copy-start | bytes 73732
  292.9 12.0 %copy-start.2 = (bf16[128,64]{0,1:T(8,128)(2,1)S(1)}, bf16[128,64]{0,1:T(8,128)(2,1)}, u32[]{:S(2)}) copy-start(bf16[128,64]{0,1:T(8,128)(2,1)} %param.17) | copy-start | bytes 49156
  292.9 12.0 %copy-start.3 = (f32[128,1]{0,1:T(1,128)S(1)}, f32[128,1]{0,1:T(1,128)}, u32[]{:S(2)}) copy-start(f32[128,1]{0,1:T(1,128)} %param.15) | copy-start | bytes 1540
  294.6 35.3 %all-to-all-start.1 = ((f32[64,8,128]{2,1,0:T(8,128)}), f32[64,8,128]{2,1,0:T(8,128)S(1)}, u32[]{:S(2)}, u32[]{:S(2)}) async-start(f32[64,8,128]{2,1,0:T(8,128)} %bitcast.15), calls=%async_computation.1 | async-start | bytes 524288 | tf_op jit(solution)/shard_map/all_to_all | solution.py:36
Sparse Core Ops, SparseCore 0:
  10.9 141.7 all-gather.4
  155.6 133.2 all-gather.2
where the time goes:
time: 339 us; the launch traced here: 337 us
  waiting for transfers between devices  140 us (41%)
  blocking collectives  88.7 us (26%)
  local copies, waits for them, and re-layouts  36 us (11%)
  matrix products  30.5 us (9%)
  starting transfers between devices  15.1 us (4%)
  between operations  14.2 us (4%)
  other arithmetic  7.34 us (2%)
  loops' own time  5.98 us (2%)
    all_gather x2, waiting for transfers between devices, in_one_piece(): filled, at, outs = (lax.all_gather(both, axis, axis=dim, tiled=True), 0, [])  140 us
    all_gather x1, blocking collectives, in_one_piece(): filled, at, outs = (lax.all_gather(both, axis, axis=dim, tiled=True), 0, [])  88.7 us
    dot_general x8, matrix products, key_step(): jnp.einsum('hqk,qhd->khd', dscore, query_part, preferred_element_type=jnp...  11 us
    all_to_all x1, starting transfers between devices, sent_and_summed(): lax.all_to_all(tiles, axis, split_axis=0, concat_axis=0, tiled=True)  10.2 us
    dot_general x8, matrix products, key_step(): jnp.einsum('hqk,qhd->khd', probs_b, grad_part, preferred_element_type=jnp...  9.58 us
    slice x10, local copies, waits for them, and re-layouts, in_one_piece(): outs.append(lax.slice_in_dim(filled, at, at + a.shape[along], axis=along))  9.3 us
    broadcast_in_dim x8, local copies, waits for them, and re-layouts, head_keys(): rotary = rot_piece[:, None, :]  7.79 us
    reshape x8, local copies, waits for them, and re-layouts, head_keys(): joined = joined_piece.reshape(piece_rows, head_count, NOPE_DIM + VALUE_DIM)  7.77 us
  transfers between devices with their start and end apart: 4, of which 2 were waited for; matrix products, arithmetic and copies ran while one was open for 21% of the time, Pallas kernels for 0%

commit v1 on v0

v1 whole, which is shorter than its diff:
```python
import math

import jax
import jax.numpy as jnp
from jax import lax
from jax.experimental import pallas as pl
from jax.experimental.pallas import tpu as pltpu
from jax.sharding import Mesh, PartitionSpec as P

NOPE_DIM = 64
ROPE_DIM = 32
VALUE_DIM = 64
HEAD_DIM = NOPE_DIM + ROPE_DIM
SCALE = HEAD_DIM**-0.5
PAD = 16
Q_ROWS = HEAD_DIM + PAD + VALUE_DIM
K_ROWS = HEAD_DIM + VALUE_DIM
BF = jnp.bfloat16
F32 = jnp.float32

FAR = ("z3", "z2", "z1")
NEAR = ("z0", "y1", "y0")
HEADS_AXIS = ("x1", "x0", "c")
GROUP = 8
TOK = 128


def three_parts(row):
    high = row.astype(BF)
    rest = row - high.astype(F32)
    middle = rest.astype(BF)
    low = (rest - middle.astype(F32)).astype(BF)
    return high.astype(F32), middle.astype(F32), low.astype(F32)


def prepare_keys(latents, rot_key, weight, k_out):
    joined = lax.dot_general(
        latents[...], weight[...], (((1,), (0,)), ((), ())), preferred_element_type=F32
    )
    joined_t = joined.T.astype(BF)
    block = jnp.concatenate(
        [joined_t[:NOPE_DIM], rot_key[...], joined_t[NOPE_DIM:]], axis=0
    )
    for i in range(GROUP):
        k_out[i] = block


def prepare_queries(queries, logs, outputs, grads, q_out):
    q_t = queries[...].astype(F32)
    g_t = grads[...].astype(F32)
    o_t = outputs[...].astype(F32)
    delta = jnp.sum(o_t * g_t, axis=0, keepdims=True)
    rows = three_parts(logs[...] * (-1.0 / SCALE)) + three_parts(-delta)
    index = lax.broadcasted_iota(jnp.int32, (PAD, TOK), 0)
    pad = jnp.zeros((PAD, TOK), F32)
    for i, row in enumerate(rows):
        pad = jnp.where(index == i, row, pad)
    block = jnp.concatenate([q_t, pad, g_t], axis=0).astype(BF)
    for i in range(GROUP):
        q_out[i] = block


def attend(q_all, k_all, dq_out, dkv_out, q_t, q_tok, g_tok, k_t, k_tok, v_tok, dq_acc, dk_acc, dv_acc):
    total = GROUP * TOK
    lane = lax.broadcasted_iota(jnp.int32, (TOK, PAD), 1)
    key_pad = jnp.where(lane < 3, 1.0, 0.0).astype(F32)
    value_pad = jnp.where((lane >= 3) & (lane < 6), 1.0, 0.0).astype(F32)
    for i in range(GROUP):
        at = slice(i * TOK, (i + 1) * TOK)
        q_block = q_all[i]
        q_t[:, at] = q_block
        tok = q_block.astype(F32).T
        q_tok[at, :] = tok[:, :HEAD_DIM].astype(BF)
        g_tok[at, :] = tok[:, HEAD_DIM + PAD :].astype(BF)
        k_block = k_all[i]
        k_t[:, at] = k_block[:HEAD_DIM]
        ktok = k_block.astype(F32).T
        k_tok[at, :] = jnp.concatenate([ktok[:, :HEAD_DIM], key_pad], axis=1).astype(BF)
        v_tok[at, :] = jnp.concatenate([value_pad, ktok[:, HEAD_DIM:]], axis=1).astype(BF)
    step = 256
    for qi in range(total // step):
        qs = slice(qi * step, (qi + 1) * step)
        for ki in range(total // step):
            ks = slice(ki * step, (ki + 1) * step)
            scores = jnp.dot(k_tok[ks, :], q_t[: HEAD_DIM + PAD, qs], preferred_element_type=F32)
            probs = jnp.exp2(scores * (SCALE * math.log2(math.e)))
            dprob = jnp.dot(v_tok[ks, :], q_t[HEAD_DIM:, qs], preferred_element_type=F32)
            dscore = (probs * dprob).astype(BF)
            dk = jnp.dot(dscore, q_tok[qs, :], preferred_element_type=F32)
            dv = jnp.dot(probs.astype(BF), g_tok[qs, :], preferred_element_type=F32)
            dq = jnp.dot(k_t[:, ks], dscore, preferred_element_type=F32)
            if qi == 0:
                dk_acc[ks, :] = dk
                dv_acc[ks, :] = dv
            else:
                dk_acc[ks, :] += dk
                dv_acc[ks, :] += dv
            if ki == 0:
                dq_acc[:, qs] = dq
            else:
                dq_acc[:, qs] += dq
    for i in range(GROUP):
        at = slice(i * TOK, (i + 1) * TOK)
        dq_out[i] = (dq_acc[:, at] * SCALE).astype(BF)
        dkv_out[i] = jnp.concatenate(
            [(dk_acc[at, :] * SCALE).T, dv_acc[at, :].T], axis=0
        ).astype(BF)


def finish_keys(dkv, key_grad, value_grad, stacked_out, rot_out):
    total = dkv[0].astype(F32)
    for i in range(1, GROUP):
        total = total + dkv[i].astype(F32)
    rot = total[NOPE_DIM:HEAD_DIM]
    stacked_t = jnp.concatenate([total[:NOPE_DIM], total[HEAD_DIM:]], axis=0)
    stacked_out[...] = stacked_t.T.astype(BF)
    key_grad[...] = total[:NOPE_DIM].astype(BF)
    value_grad[...] = total[HEAD_DIM:].astype(BF)
    for i in range(GROUP):
        rot_out[i] = rot


def weigh(stacked, latents, weight_out):
    weight = lax.dot_general(
        latents[...], stacked[...], (((0,), (0,)), ((), ())), preferred_element_type=F32
    )
    by_owner = weight.reshape(GROUP, GROUP, 8, TOK)
    for i in range(GROUP):
        weight_out[i] = by_owner[:, i].reshape(GROUP * 8, TOK).astype(BF)


def join_far(weight, dq, far_out):
    total = weight[0].astype(F32)
    for i in range(1, GROUP):
        total = total + weight[i].astype(F32)
    for i in range(GROUP):
        rows = total[i * 8 : (i + 1) * 8]
        high = rows.astype(BF).astype(F32)
        far_out[i, :HEAD_DIM] = dq[i]
        far_out[i, HEAD_DIM:] = jnp.concatenate([high, rows - high], axis=0).astype(BF)


def finish_rest(far, rot, query_grad, weight_grad, rot_grad):
    total = far[0].astype(F32)
    around = rot[0]
    for i in range(1, GROUP):
        total = total + far[i].astype(F32)
        around = around + rot[i]
    query_grad[...] = total[:HEAD_DIM].astype(BF)
    weight_grad[...] = total[HEAD_DIM : HEAD_DIM + 8] + total[HEAD_DIM + 8 :]
    rot_grad[...] = around


def call(body, args, outs, name, scratch=()):
    shapes = [
        pltpu.VMEM(shape, kind) if near else jax.ShapeDtypeStruct(shape, kind)
        for shape, kind, near in outs
    ]
    return pl.pallas_call(body, out_shape=shapes, scratch_shapes=list(scratch), name=name)(*args)


def close(x):
    return pltpu.with_memory_space_constraint(x, pltpu.VMEM)


def exchange(x, axes):
    return close(lax.all_to_all(x, axes, split_axis=0, concat_axis=0, tiled=True))


def per_device(queries, latents, rot_key, kv_weight, log_sums, outputs, out_grad):
    total = GROUP * TOK
    (k_send,) = call(
        prepare_keys,
        (latents, rot_key.T, kv_weight),
        [((GROUP, K_ROWS, TOK), BF, True)],
        "prepare_keys",
    )
    (q_send,) = call(
        prepare_queries,
        (queries.T, log_sums.T, outputs.T, out_grad.T),
        [((GROUP, Q_ROWS, TOK), BF, True)],
        "prepare_queries",
    )
    k_all = exchange(k_send, NEAR)
    q_all = exchange(q_send, FAR)
    dq, dkv = call(
        attend,
        (q_all, k_all),
        [((GROUP, HEAD_DIM, TOK), BF, True), ((GROUP, K_ROWS, TOK), BF, True)],
        "attend",
        [
            pltpu.VMEM((Q_ROWS, total), BF),
            pltpu.VMEM((total, HEAD_DIM), BF),
            pltpu.VMEM((total, VALUE_DIM), BF),
            pltpu.VMEM((HEAD_DIM, total), BF),
            pltpu.VMEM((total, HEAD_DIM + PAD), BF),
            pltpu.VMEM((total, PAD + VALUE_DIM), BF),
            pltpu.VMEM((HEAD_DIM, total), F32),
            pltpu.VMEM((total, HEAD_DIM), F32),
            pltpu.VMEM((total, VALUE_DIM), F32),
        ],
    )
    key_grad, value_grad, stacked, rot_send = call(
        finish_keys,
        (exchange(dkv, NEAR),),
        [
            ((NOPE_DIM, TOK), BF, False),
            ((VALUE_DIM, TOK), BF, False),
            ((TOK, NOPE_DIM + VALUE_DIM), BF, True),
            ((GROUP, ROPE_DIM, TOK), F32, True),
        ],
        "finish_keys",
    )
    rot_all = exchange(rot_send, HEADS_AXIS)
    (weight_send,) = call(
        weigh, (close(stacked), latents), [((GROUP, GROUP * 8, TOK), BF, True)], "weigh"
    )
    (far_send,) = call(
        join_far,
        (exchange(weight_send, NEAR), close(dq)),
        [((GROUP, HEAD_DIM + 16, TOK), BF, True)],
        "join_far",
    )
    query_grad, weight_grad, rot_grad = call(
        finish_rest,
        (exchange(far_send, FAR), rot_all),
        [((HEAD_DIM, TOK), BF, False), ((8, TOK), F32, False), ((ROPE_DIM, TOK), F32, False)],
        "finish_rest",
    )
    return query_grad.T, key_grad.T, value_grad.T, rot_grad.T, weight_grad


def solution(mesh):
    sp, tp = FAR + NEAR, HEADS_AXIS
    split = Mesh(mesh.devices.reshape((2,) * 9), sp + tp)
    placed = (P(sp, tp), P(sp, None), P(sp, None), P(None, tp), P(sp, tp), P(sp, tp), P(sp, tp))
    return jax.shard_map(
        per_device,
        mesh=split,
        in_specs=placed,
        out_specs=(P(sp, tp), P(sp, tp), P(sp, tp), P(sp, None), P(sp, tp)),
        check_vma=False,
    )
```

time: 339 us -> 114 us (0.34)
  waiting for transfers between devices: 140 us -> 11 us
  local copies, waits for them, and re-layouts: 36 us -> 0 us
  matrix products: 30.5 us -> 0 us
  between operations: 14.2 us -> 0.65 us
  Pallas kernels: 0 us -> 9.65 us
  blocking collectives: 88.7 us -> 80.5 us
  other arithmetic: 7.34 us -> 0 us
  loops' own time: 5.98 us -> 0 us
  starting transfers between devices: 15.1 us -> 10.6 us
    all_gather x2 -> x0, waiting for transfers between devices: 140 us -> none  [in_one_piece(): filled, at, outs = (lax.all_gather(both, axis, axis=dim, tiled=True), 0, [])]
    all_gather x1 -> x0, blocking collectives: 88.7 us -> none  [in_one_piece(): filled, at, outs = (lax.all_gather(both, axis, axis=dim, tiled=True), 0, [])]
    all_to_all x0 -> x4, blocking collectives: none -> 80.5 us  [exchange(): lax.all_to_all(x, axes, split_axis=0, concat_axis=0, tiled=True)]
    dot_general x42 -> x0, matrix products: 30.5 us -> none  [the longest x8 11 us: key_step(): jnp.einsum('hqk,qhd->khd', dscore, query_part, preferred_element_type=jnp...]
    all_to_all x2, waiting for transfers between devices: 0.01 us -> 11 us  [exchange(): lax.all_to_all(x, axes, split_axis=0, concat_axis=0, tiled=True)]
    pallas_call x0 -> x7, Pallas kernels: none -> 9.65 us  [call(): pl.pallas_call(body, out_shape=shapes, scratch_shapes=list(scratch), name...]
    slice x12 -> x0, local copies, waits for them, and re-layouts: 9.31 us -> none  [the longest x10 9.3 us: in_one_piece(): outs.append(lax.slice_in_dim(filled, at, at + a.shape[along], axis=along))]
    broadcast_in_dim x9 -> x0, local copies, waits for them, and re-layouts: 8.45 us -> none  [the longest x8 7.79 us: head_keys(): rotary = rot_piece[:, None, :]]
  transfers between devices with their start and end apart: 4 -> 2, of which waited for: 2 -> 2; matrix products, arithmetic and copies ran while one was open for 21% -> 0% of each run, Pallas kernels for 0% -> 1%
where the time goes in v1:
time: 114 us; the launch traced here: 112 us
  blocking collectives  80.5 us (71%)
  waiting for transfers between devices  11 us (10%)
  starting transfers between devices  10.6 us (9%)
  Pallas kernels  9.65 us (8%)
    all_to_all x4, blocking collectives, exchange(): lax.all_to_all(x, axes, split_axis=0, concat_axis=0, tiled=True)  80.5 us
    all_to_all x2, waiting for transfers between devices, exchange(): lax.all_to_all(x, axes, split_axis=0, concat_axis=0, tiled=True)  11 us
    all_to_all x2, starting transfers between devices, exchange(): lax.all_to_all(x, axes, split_axis=0, concat_axis=0, tiled=True)  10.6 us
    pallas_call x7, Pallas kernels, call(): pl.pallas_call(body, out_shape=shapes, scratch_shapes=list(scratch), name...  9.65 us
  transfers between devices with their start and end apart: 2, of which 2 were waited for; matrix products, arithmetic and copies ran while one was open for 0% of the time, Pallas kernels for 1%

profile of v1, /device:TPU:6, one launch (start us, length us, event | category | flops | bytes accessed | tf_op | source)
XLA Modules:
  0.0 112.4 jit_solution(18015553332297578326)
XLA Ops:
  0.6 2.0 %prepare_keys.1 = bf16[8,160,128]{2,1,0:T(8,128)(2,1)} custom-call(bf16[128,512]{1,0:T(8,128)(2,1)} %latents.3, bf16[32,128]{1,0:T(8,128)(2,1)} %bitcast.12, bf16[512,128]{1,0:T(8,128)(2,1)} %weight.1), custom_call_target="tpu_custom_call" | custom-call | tf_op jit(solution)/shard_map/prepare_keys/pallas_call | solution.py:159
  2.6 5.8 %all-to-all-start.1 = ((bf16[8,160,128]{2,1,0:T(8,128)(2,1)}), bf16[8,160,128]{2,1,0:T(8,128)(2,1)S(1)}, u32[]{:S(2)}, u32[]{:S(2)}) async-start(bf16[8,160,128]{2,1,0:T(8,128)(2,1)} %prepare_keys.1), calls=%async_computation.1 | async-start | bytes 655360 | tf_op jit(solution)/shard_map/all_to_all | solution.py:167
  8.4 0.8 prepare_queries.1
  9.2 7.0 %all-to-all-done.1.k_all = bf16[8,160,128]{2,1,0:T(8,128)(2,1)S(1)} async-done(((bf16[8,160,128]{2,1,0:T(8,128)(2,1)}), bf16[8,160,128]{2,1,0:T(8,128)(2,1)S(1)}, u32[]{:S(2)}, u32[]{:S(2)}) %all-to-all-start.1) | async-done | bytes 327712 | tf_op jit(solution)/shard_map/all_to_all | solution.py:167
  16.3 38.1 %all_to_all.30.q_all = bf16[8,176,128]{2,1,0:T(8,128)(2,1)S(1)} all-to-all(bf16[8,176,128]{2,1,0:T(8,128)(2,1)S(1)} %prepare_queries.1), channel_id=1, replica_groups=mesh['z3'=2,'z2'=2,'z1'=2,'z0'=2,'y1'=2,'y0'=2,'x1'=2,'x0'=2,'c'=2] {'z3..., dimensions={0} | all-to-all | bytes 720896 | tf_op jit(solution)/shard_map/all_to_all | solution.py:167
  54.4 4.4 %attend.1 = (bf16[8,96,128]{2,1,0:T(8,128)(2,1)S(1)}, bf16[8,160,128]{2,1,0:T(8,128)(2,1)S(1)}) custom-call(bf16[8,176,128]{2,1,0:T(8,128)(2,1)S(1)} %all_to_all.30.q_all, bf16[8,160,128]{2,1,0:T(8,128)(2,1)S(1)} %all-to-all-done.1.k_all), custom_call_target="tpu_custom_call" | custom-call | tf_op jit(solution)/shard_map/attend/pallas_call | solution.py:159
  58.8 10.9 %all_to_all.31.dkv = bf16[8,160,128]{2,1,0:T(8,128)(2,1)S(1)} all-to-all(bf16[8,160,128]{2,1,0:T(8,128)(2,1)S(1)} %get-tuple-element.14), channel_id=1, replica_groups=mesh['z3'=2,'z2'=2,'z1'=2,'z0'=2,'y1'=2,'y0'=2,'x1'=2,'x0'=2,'c'=2] {'z0..., dimensions={0} | all-to-all | bytes 655360 | tf_op jit(solution)/shard_map/all_to_all | solution.py:167
  69.7 0.7 finish_keys.1
  70.4 1.1 weigh.1
  71.5 9.0 %all_to_all.32.weight = bf16[8,64,128]{2,1,0:T(8,128)(2,1)S(1)} all-to-all(bf16[8,64,128]{2,1,0:T(8,128)(2,1)S(1)} %weigh.1), channel_id=1, replica_groups=mesh['z3'=2,'z2'=2,'z1'=2,'z0'=2,'y1'=2,'y0'=2,'x1'=2,'x0'=2,'c'=2] {'z0..., dimensions={0} | all-to-all | bytes 262144 | tf_op jit(solution)/shard_map/all_to_all | solution.py:167
  80.5 4.8 %all-to-all-start.5 = ((f32[8,32,128]{2,1,0:T(8,128)}), f32[8,32,128]{2,1,0:T(8,128)S(1)}, u32[]{:S(2)}, u32[]{:S(2)}) async-start(f32[8,32,128]{2,1,0:T(8,128)} %get-tuple-element.17), calls=%async_computation.5 | async-start | bytes 262144 | tf_op jit(solution)/shard_map/all_to_all | solution.py:167
  85.3 4.0 %all-to-all-done.5.rot = f32[8,32,128]{2,1,0:T(8,128)S(1)} async-done(((f32[8,32,128]{2,1,0:T(8,128)}), f32[8,32,128]{2,1,0:T(8,128)S(1)}, u32[]{:S(2)}, u32[]{:S(2)}) %all-to-all-start.5) | async-done | bytes 131104 | tf_op jit(solution)/shard_map/all_to_all | solution.py:167
  89.3 22.5 %all_to_all.33.far = bf16[8,112,128]{2,1,0:T(8,128)(2,1)S(1)} all-to-all(bf16[8,112,128]{2,1,0:T(8,128)(2,1)S(1)} %join_far.1), channel_id=1, replica_groups=mesh['z3'=2,'z2'=2,'z1'=2,'z0'=2,'y1'=2,'y0'=2,'x1'=2,'x0'=2,'c'=2] {'z3..., dimensions={0} | all-to-all | bytes 458752 | tf_op jit(solution)/shard_map/all_to_all | solution.py:167
  111.8 0.6 finish_rest.1
  (1 shorter events, 0.0 us)
Async XLA Ops:
  2.6 13.7 %all-to-all-start.1 = ((bf16[8,160,128]{2,1,0:T(8,128)(2,1)}), bf16[8,160,128]{2,1,0:T(8,128)(2,1)S(1)}, u32[]{:S(2)}, u32[]{:S(2)}) async-start(bf16[8,160,128]{2,1,0:T(8,128)(2,1)} %prepare_keys.1), calls=%async_computation.1 | async-start | bytes 655360 | tf_op jit(solution)/shard_map/all_to_all | solution.py:167
  80.5 8.8 %all-to-all-start.5 = ((f32[8,32,128]{2,1,0:T(8,128)}), f32[8,32,128]{2,1,0:T(8,128)S(1)}, u32[]{:S(2)}, u32[]{:S(2)}) async-start(f32[8,32,128]{2,1,0:T(8,128)} %get-tuple-element.17), calls=%async_computation.5 | async-start | bytes 262144 | tf_op jit(solution)/shard_map/all_to_all | solution.py:167

commit v2 on v1

--- a/solution.py
+++ b/solution.py
@@ -19,7 +19,7 @@
 F32 = jnp.float32
 
 FAR = ("z3", "z2", "z1")
-NEAR = ("z0", "y1", "y0")
+NEAR = ("y1", "y0", "z0")
 HEADS_AXIS = ("x1", "x0", "c")
 GROUP = 8
 TOK = 128
@@ -41,8 +41,7 @@
     block = jnp.concatenate(
         [joined_t[:NOPE_DIM], rot_key[...], joined_t[NOPE_DIM:]], axis=0
     )
-    for i in range(GROUP):
-        k_out[i] = block
+    k_out[...] = block
 
 
 def prepare_queries(queries, logs, outputs, grads, q_out):
@@ -116,8 +115,7 @@
     stacked_out[...] = stacked_t.T.astype(BF)
     key_grad[...] = total[:NOPE_DIM].astype(BF)
     value_grad[...] = total[HEAD_DIM:].astype(BF)
-    for i in range(GROUP):
-        rot_out[i] = rot
+    rot_out[...] = rot
 
 
 def weigh(stacked, latents, weight_out):
@@ -126,7 +124,8 @@
     )
     by_owner = weight.reshape(GROUP, GROUP, 8, TOK)
     for i in range(GROUP):
-        weight_out[i] = by_owner[:, i].reshape(GROUP * 8, TOK).astype(BF)
+        owner = (i % 2) * 4 + i // 2
+        weight_out[i] = by_owner[:, owner].reshape(GROUP * 8, TOK).astype(BF)
 
 
 def join_far(weight, dq, far_out):
@@ -167,12 +166,18 @@
     return close(lax.all_to_all(x, axes, split_axis=0, concat_axis=0, tiled=True))
 
 
+def gather_pairs(x, axes):
+    for axis in axes:
+        x = lax.all_gather(x, axis, axis=0)
+    return close(x.reshape((GROUP,) + x.shape[len(axes) :]))
+
+
 def per_device(queries, latents, rot_key, kv_weight, log_sums, outputs, out_grad):
     total = GROUP * TOK
     (k_send,) = call(
         prepare_keys,
         (latents, rot_key.T, kv_weight),
-        [((GROUP, K_ROWS, TOK), BF, True)],
+        [((K_ROWS, TOK), BF, True)],
         "prepare_keys",
     )
     (q_send,) = call(
@@ -181,7 +186,7 @@
         [((GROUP, Q_ROWS, TOK), BF, True)],
         "prepare_queries",
     )
-    k_all = exchange(k_send, NEAR)
+    k_all = gather_pairs(k_send, NEAR[::-1])
     q_all = exchange(q_send, FAR)
     dq, dkv = call(
         attend,
@@ -207,11 +212,11 @@
             ((NOPE_DIM, TOK), BF, False),
             ((VALUE_DIM, TOK), BF, False),
             ((TOK, NOPE_DIM + VALUE_DIM), BF, True),
-            ((GROUP, ROPE_DIM, TOK), F32, True),
+            ((ROPE_DIM, TOK), F32, True),
         ],
         "finish_keys",
     )
-    rot_all = exchange(rot_send, HEADS_AXIS)
+    rot_all = gather_pairs(rot_send, HEADS_AXIS[::-1])
     (weight_send,) = call(
         weigh, (close(stacked), latents), [((GROUP, GROUP * 8, TOK), BF, True)], "weigh"
     )
@@ -231,7 +236,7 @@
 
 
 def solution(mesh):
-    sp, tp = FAR + NEAR, HEADS_AXIS
+    sp, tp = FAR + ("z0", "y1", "y0"), HEADS_AXIS
     split = Mesh(mesh.devices.reshape((2,) * 9), sp + tp)
     placed = (P(sp, tp), P(sp, None), P(sp, None), P(None, tp), P(sp, tp), P(sp, tp), P(sp, tp))
     return jax.shard_map(

time: 114 us -> 105 us (0.921)
  blocking collectives: 80.5 us -> 61.5 us
  starting transfers between devices: 10.6 us -> 28.6 us
  waiting for transfers between devices: 11 us -> 3.25 us
    all_to_all x4 -> x2, blocking collectives: 80.5 us -> 21.8 us  [exchange(): lax.all_to_all(x, axes, split_axis=0, concat_axis=0, tiled=True)]
    all_gather x0 -> x6, blocking collectives: none -> 39.7 us  [gather_pairs(): x = lax.all_gather(x, axis, axis=0)]
    all_to_all x2, starting transfers between devices: 10.6 us -> 28.6 us  [exchange(): lax.all_to_all(x, axes, split_axis=0, concat_axis=0, tiled=True)]
    all_to_all x2, waiting for transfers between devices: 11 us -> 3.25 us  [exchange(): lax.all_to_all(x, axes, split_axis=0, concat_axis=0, tiled=True)]
  transfers between devices with their start and end apart: 2 -> 2, of which waited for: 2 -> 1; matrix products, arithmetic and copies ran while one was open for 0% -> 0% of each run, Pallas kernels for 1% -> 1%
where the time goes in v2:
time: 105 us; the launch traced here: 104 us
  blocking collectives  61.5 us (59%)
  starting transfers between devices  28.6 us (27%)
  Pallas kernels  10.3 us (10%)
  waiting for transfers between devices  3.25 us (3%)
    all_gather x6, blocking collectives, gather_pairs(): x = lax.all_gather(x, axis, axis=0)  39.7 us
    all_to_all x2, starting transfers between devices, exchange(): lax.all_to_all(x, axes, split_axis=0, concat_axis=0, tiled=True)  28.6 us
    all_to_all x2, blocking collectives, exchange(): lax.all_to_all(x, axes, split_axis=0, concat_axis=0, tiled=True)  21.8 us
    pallas_call x7, Pallas kernels, call(): pl.pallas_call(body, out_shape=shapes, scratch_shapes=list(scratch), name...  10.3 us
    all_to_all x2, waiting for transfers between devices, exchange(): lax.all_to_all(x, axes, split_axis=0, concat_axis=0, tiled=True)  3.25 us
  transfers between devices with their start and end apart: 2, of which 1 were waited for; matrix products, arithmetic and copies ran while one was open for 0% of the time, Pallas kernels for 1%

profile of v2, /device:TPU:6, one launch (start us, length us, event | category | flops | bytes accessed | tf_op | source)
XLA Modules:
  0.0 104.3 jit_solution(7872046175242167598)
XLA Ops:
  0.6 1.6 %prepare_queries.1 = bf16[8,176,128]{2,1,0:T(8,128)(2,1)} custom-call(bf16[96,128]{1,0:T(8,128)(2,1)} %bitcast.21, f32[1,128]{1,0:T(1,128)} %bitcast.25, bf16[64,128]{1,0:T(8,128)(2,1)} %bitcast.22, bf16[64,128]{1,0:T(8,128)(2,1)} %bitcast.23), custom_call_target="tpu_custom_call" | custom-call | tf_op jit(solution)/shard_map/prepare_queries/pallas_call | solution.py:158
  2.2 15.1 %all-to-all-start = ((bf16[8,176,128]{2,1,0:T(8,128)(2,1)}), bf16[8,176,128]{2,1,0:T(8,128)(2,1)S(1)}, u32[]{:S(2)}, u32[]{:S(2)}) async-start(bf16[8,176,128]{2,1,0:T(8,128)(2,1)} %prepare_queries.1), calls=%async_computation | async-start | bytes 720896 | tf_op jit(solution)/shard_map/all_to_all | solution.py:166
  17.3 1.2 %prepare_keys.1 = bf16[160,128]{1,0:T(8,128)(2,1)S(1)} custom-call(bf16[128,512]{1,0:T(8,128)(2,1)} %latents.3, bf16[32,128]{1,0:T(8,128)(2,1)} %bitcast.24, bf16[512,128]{1,0:T(8,128)(2,1)} %weight.1), custom_call_target="tpu_custom_call" | custom-call | tf_op jit(solution)/shard_map/prepare_keys/pallas_call | solution.py:158
  18.5 14.3 %all-gather = bf16[320,128]{1,0:T(8,128)(2,1)S(1)} all-gather(bf16[160,128]{1,0:T(8,128)(2,1)S(1)} %prepare_keys.1), channel_id=2, replica_groups=mesh['z3'=2,'z2'=2,'z1'=2,'z0'=2,'y1'=2,'y0'=2,'x1'=2,'x0'=2,'c'=2] {'z0'}, dimensions={0}, use_global_device_ids=true | all-gather | bytes 122880 | tf_op jit(solution)/shard_map/all_gather | solution.py:171
  32.8 5.1 %all-gather.1 = bf16[4,160,128]{2,1,0:T(8,128)(2,1)S(1)} all-gather(bf16[2,160,128]{2,1,0:T(8,128)(2,1)S(1)} %bitcast.18), channel_id=3, replica_groups=mesh['z3'=2,'z2'=2,'z1'=2,'z0'=2,'y1'=2,'y0'=2,'x1'=2,'x0'=2,'c'=2] {'y0'}, dimensions={0}, use_global_device_ids=true | all-gather | bytes 245760 | tf_op jit(solution)/shard_map/all_gather | solution.py:171
  37.9 7.5 %all-gather.2 = bf16[4,2,160,128]{3,2,1,0:T(8,128)(2,1)S(1)} all-gather(bf16[2,2,160,128]{3,2,1,0:T(8,128)(2,1)S(1)} %bitcast.17), channel_id=4, replica_groups=mesh['z3'=2,'z2'=2,'z1'=2,'z0'=2,'y1'=2,'y0'=2,'x1'=2,'x0'=2,'c'=2] {'y1'}, dimensions={0}, use_global_device_ids=true | all-gather | bytes 491520 | tf_op jit(solution)/shard_map/all_gather | solution.py:171
  45.4 0.0 all-to-all-done.q_all
  45.4 4.4 %attend.1 = (bf16[8,96,128]{2,1,0:T(8,128)(2,1)S(1)}, bf16[8,160,128]{2,1,0:T(8,128)(2,1)S(1)}) custom-call(bf16[8,176,128]{2,1,0:T(8,128)(2,1)S(1)} %all-to-all-done.q_all, bf16[8,160,128]{2,1,0:T(8,128)(2,1)S(1)} %bitcast.15), custom_call_target="tpu_custom_call" | custom-call | tf_op jit(solution)/shard_map/attend/pallas_call | solution.py:158
  49.8 12.7 %all_to_all.20.dkv = bf16[8,160,128]{2,1,0:T(8,128)(2,1)S(1)} all-to-all(bf16[8,160,128]{2,1,0:T(8,128)(2,1)S(1)} %get-tuple-element.14), channel_id=1, replica_groups=mesh['z3'=2,'z2'=2,'z1'=2,'z0'=2,'y1'=2,'y0'=2,'x1'=2,'x0'=2,'c'=2] {'y1..., dimensions={0} | all-to-all | bytes 655360 | tf_op jit(solution)/shard_map/all_to_all | solution.py:166
  62.5 0.7 finish_keys.1
  63.1 1.1 %weigh.1 = bf16[8,64,128]{2,1,0:T(8,128)(2,1)S(1)} custom-call(bf16[128,128]{1,0:T(8,128)(2,1)S(1)} %get-tuple-element.15.stacked, bf16[128,512]{1,0:T(8,128)(2,1)} %latents.3), custom_call_target="tpu_custom_call" | custom-call | tf_op jit(solution)/shard_map/weigh/pallas_call | solution.py:158
  64.3 9.1 %all_to_all.21.weight = bf16[8,64,128]{2,1,0:T(8,128)(2,1)S(1)} all-to-all(bf16[8,64,128]{2,1,0:T(8,128)(2,1)S(1)} %weigh.1), channel_id=1, replica_groups=mesh['z3'=2,'z2'=2,'z1'=2,'z0'=2,'y1'=2,'y0'=2,'x1'=2,'x0'=2,'c'=2] {'y1..., dimensions={0} | all-to-all | bytes 262144 | tf_op jit(solution)/shard_map/all_to_all | solution.py:166
  73.4 0.7 join_far.1
  74.1 13.5 %all-to-all-start.3 = ((bf16[8,112,128]{2,1,0:T(8,128)(2,1)}), bf16[8,112,128]{2,1,0:T(8,128)(2,1)S(1)}, u32[]{:S(2)}, u32[]{:S(2)}) async-start(bf16[8,112,128]{2,1,0:T(8,128)(2,1)} %join_far.1), calls=%async_computation.3 | async-start | bytes 458752 | tf_op jit(solution)/shard_map/all_to_all | solution.py:166
  87.6 1.8 %all-gather.3 = f32[64,128]{1,0:T(8,128)S(1)} all-gather(f32[32,128]{1,0:T(8,128)S(1)} %get-tuple-element.17), channel_id=5, replica_groups=mesh['z3'=2,'z2'=2,'z1'=2,'z0'=2,'y1'=2,'y0'=2,'x1'=2,'x0'=2,'c'=2] {'c'}, dimensions={0}, use_global_device_ids=true | all-gather | bytes 49152 | tf_op jit(solution)/shard_map/all_gather | solution.py:171
  89.4 4.6 %all-gather.4 = f32[4,32,128]{2,1,0:T(8,128)S(1)} all-gather(f32[2,32,128]{2,1,0:T(8,128)S(1)} %bitcast.20), channel_id=6, replica_groups=mesh['z3'=2,'z2'=2,'z1'=2,'z0'=2,'y1'=2,'y0'=2,'x1'=2,'x0'=2,'c'=2] {'x0'}, dimensions={0}, use_global_device_ids=true | all-gather | bytes 98304 | tf_op jit(solution)/shard_map/all_gather | solution.py:171
  94.0 6.4 %all-gather.5 = f32[4,2,32,128]{3,2,1,0:T(8,128)S(1)} all-gather(f32[2,2,32,128]{3,2,1,0:T(8,128)S(1)} %bitcast.19), channel_id=7, replica_groups=mesh['z3'=2,'z2'=2,'z1'=2,'z0'=2,'y1'=2,'y0'=2,'x1'=2,'x0'=2,'c'=2] {'x1'}, dimensions={0}, use_global_device_ids=true | all-gather | bytes 196608 | tf_op jit(solution)/shard_map/all_gather | solution.py:171
  100.4 3.2 %all-to-all-done.3.far = bf16[8,112,128]{2,1,0:T(8,128)(2,1)S(1)} async-done(((bf16[8,112,128]{2,1,0:T(8,128)(2,1)}), bf16[8,112,128]{2,1,0:T(8,128)(2,1)S(1)}, u32[]{:S(2)}, u32[]{:S(2)}) %all-to-all-start.3) | async-done | bytes 229408 | tf_op jit(solution)/shard_map/all_to_all | solution.py:166
  103.6 0.6 finish_rest.1
Async XLA Ops:
  2.2 43.2 %all-to-all-start = ((bf16[8,176,128]{2,1,0:T(8,128)(2,1)}), bf16[8,176,128]{2,1,0:T(8,128)(2,1)S(1)}, u32[]{:S(2)}, u32[]{:S(2)}) async-start(bf16[8,176,128]{2,1,0:T(8,128)(2,1)} %prepare_queries.1), calls=%async_computation | async-start | bytes 720896 | tf_op jit(solution)/shard_map/all_to_all | solution.py:166
  74.1 29.5 %all-to-all-start.3 = ((bf16[8,112,128]{2,1,0:T(8,128)(2,1)}), bf16[8,112,128]{2,1,0:T(8,128)(2,1)S(1)}, u32[]{:S(2)}, u32[]{:S(2)}) async-start(bf16[8,112,128]{2,1,0:T(8,128)(2,1)} %join_far.1), calls=%async_computation.3 | async-start | bytes 458752 | tf_op jit(solution)/shard_map/all_to_all | solution.py:166

commit v3 on v2

--- a/solution.py
+++ b/solution.py
@@ -19,7 +19,7 @@
 F32 = jnp.float32
 
 FAR = ("z3", "z2", "z1")
-NEAR = ("y1", "y0", "z0")
+NEAR = ("z0", "y1", "y0")
 HEADS_AXIS = ("x1", "x0", "c")
 GROUP = 8
 TOK = 128
@@ -59,7 +59,7 @@
         q_out[i] = block
 
 
-def attend(q_all, k_all, dq_out, dkv_out, q_t, q_tok, g_tok, k_t, k_tok, v_tok, dq_acc, dk_acc, dv_acc):
+def attend(q_all, k_all, dq_out, dkv_out, q_t, q_tok, g_tok, k_t, k_tok, v_tok, dq_acc, dk_acc, dv_acc, dscores, probs_b):
     total = GROUP * TOK
     lane = lax.broadcasted_iota(jnp.int32, (TOK, PAD), 1)
     key_pad = jnp.where(lane < 3, 1.0, 0.0).astype(F32)
@@ -77,27 +77,20 @@
         k_tok[at, :] = jnp.concatenate([ktok[:, :HEAD_DIM], key_pad], axis=1).astype(BF)
         v_tok[at, :] = jnp.concatenate([value_pad, ktok[:, HEAD_DIM:]], axis=1).astype(BF)
     step = 256
-    for qi in range(total // step):
-        qs = slice(qi * step, (qi + 1) * step)
-        for ki in range(total // step):
-            ks = slice(ki * step, (ki + 1) * step)
+    for ki in range(total // step):
+        ks = slice(ki * step, (ki + 1) * step)
+        for qi in range(total // step):
+            qs = slice(qi * step, (qi + 1) * step)
             scores = jnp.dot(k_tok[ks, :], q_t[: HEAD_DIM + PAD, qs], preferred_element_type=F32)
             probs = jnp.exp2(scores * (SCALE * math.log2(math.e)))
             dprob = jnp.dot(v_tok[ks, :], q_t[HEAD_DIM:, qs], preferred_element_type=F32)
-            dscore = (probs * dprob).astype(BF)
-            dk = jnp.dot(dscore, q_tok[qs, :], preferred_element_type=F32)
-            dv = jnp.dot(probs.astype(BF), g_tok[qs, :], preferred_element_type=F32)
-            dq = jnp.dot(k_t[:, ks], dscore, preferred_element_type=F32)
-            if qi == 0:
-                dk_acc[ks, :] = dk
-                dv_acc[ks, :] = dv
-            else:
-                dk_acc[ks, :] += dk
-                dv_acc[ks, :] += dv
-            if ki == 0:
-                dq_acc[:, qs] = dq
-            else:
-                dq_acc[:, qs] += dq
+            dscores[ks, qs] = (probs * dprob).astype(BF)
+            probs_b[ks, qs] = probs.astype(BF)
+        dk_acc[ks, :] = jnp.dot(dscores[ks, :], q_tok[...], preferred_element_type=F32)
+        dv_acc[ks, :] = jnp.dot(probs_b[ks, :], g_tok[...], preferred_element_type=F32)
+    for qi in range(total // step):
+        qs = slice(qi * step, (qi + 1) * step)
+        dq_acc[:, qs] = jnp.dot(k_t[...], dscores[:, qs], preferred_element_type=F32)
     for i in range(GROUP):
         at = slice(i * TOK, (i + 1) * TOK)
         dq_out[i] = (dq_acc[:, at] * SCALE).astype(BF)
@@ -106,26 +99,20 @@
         ).astype(BF)
 
 
-def finish_keys(dkv, key_grad, value_grad, stacked_out, rot_out):
+def finish_keys(dkv, latents, key_grad, value_grad, rot_out, weight_out):
     total = dkv[0].astype(F32)
     for i in range(1, GROUP):
         total = total + dkv[i].astype(F32)
-    rot = total[NOPE_DIM:HEAD_DIM]
-    stacked_t = jnp.concatenate([total[:NOPE_DIM], total[HEAD_DIM:]], axis=0)
-    stacked_out[...] = stacked_t.T.astype(BF)
+    rot_out[...] = total[NOPE_DIM:HEAD_DIM]
     key_grad[...] = total[:NOPE_DIM].astype(BF)
     value_grad[...] = total[HEAD_DIM:].astype(BF)
-    rot_out[...] = rot
-
-
-def weigh(stacked, latents, weight_out):
+    stacked = jnp.concatenate([total[:NOPE_DIM], total[HEAD_DIM:]], axis=0).T.astype(BF)
     weight = lax.dot_general(
-        latents[...], stacked[...], (((0,), (0,)), ((), ())), preferred_element_type=F32
+        latents[...], stacked, (((0,), (0,)), ((), ())), preferred_element_type=F32
     )
     by_owner = weight.reshape(GROUP, GROUP, 8, TOK)
     for i in range(GROUP):
-        owner = (i % 2) * 4 + i // 2
-        weight_out[i] = by_owner[:, owner].reshape(GROUP * 8, TOK).astype(BF)
+        weight_out[i] = by_owner[:, i].reshape(GROUP * 8, TOK).astype(BF)
 
 
 def join_far(weight, dq, far_out):
@@ -203,23 +190,22 @@
             pltpu.VMEM((HEAD_DIM, total), F32),
             pltpu.VMEM((total, HEAD_DIM), F32),
             pltpu.VMEM((total, VALUE_DIM), F32),
+            pltpu.VMEM((total, total), BF),
+            pltpu.VMEM((total, total), BF),
         ],
     )
-    key_grad, value_grad, stacked, rot_send = call(
+    key_grad, value_grad, rot_send, weight_send = call(
         finish_keys,
-        (exchange(dkv, NEAR),),
+        (exchange(dkv, NEAR), latents),
         [
             ((NOPE_DIM, TOK), BF, False),
             ((VALUE_DIM, TOK), BF, False),
-            ((TOK, NOPE_DIM + VALUE_DIM), BF, True),
             ((ROPE_DIM, TOK), F32, True),
+            ((GROUP, GROUP * 8, TOK), BF, True),
         ],
         "finish_keys",
     )
     rot_all = gather_pairs(rot_send, HEADS_AXIS[::-1])
-    (weight_send,) = call(
-        weigh, (close(stacked), latents), [((GROUP, GROUP * 8, TOK), BF, True)], "weigh"
-    )
     (far_send,) = call(
         join_far,
         (exchange(weight_send, NEAR), close(dq)),
@@ -236,7 +222,7 @@
 
 
 def solution(mesh):
-    sp, tp = FAR + ("z0", "y1", "y0"), HEADS_AXIS
+    sp, tp = FAR + NEAR, HEADS_AXIS
     split = Mesh(mesh.devices.reshape((2,) * 9), sp + tp)
     placed = (P(sp, tp), P(sp, None), P(sp, None), P(None, tp), P(sp, tp), P(sp, tp), P(sp, tp))
     return jax.shard_map(

time: 105 us -> 94.7 us (0.902)
  starting transfers between devices: 28.6 us -> 21.2 us
  blocking collectives: 61.5 us -> 54.6 us
  waiting for transfers between devices: 3.25 us -> 9.12 us
  Pallas kernels: 10.3 us -> 8.59 us
    all_to_all x2, starting transfers between devices: 28.6 us -> 21.2 us  [exchange(): lax.all_to_all(x, axes, split_axis=0, concat_axis=0, tiled=True)]
    all_gather x6, blocking collectives: 39.7 us -> 32.7 us  [gather_pairs(): x = lax.all_gather(x, axis, axis=0)]
    all_to_all x2, waiting for transfers between devices: 3.25 us -> 9.12 us  [exchange(): lax.all_to_all(x, axes, split_axis=0, concat_axis=0, tiled=True)]
    pallas_call x7 -> x6, Pallas kernels: 10.3 us -> 8.59 us  [call(): pl.pallas_call(body, out_shape=shapes, scratch_shapes=list(scratch), name...]
  transfers between devices with their start and end apart: 2 -> 2, of which waited for: 1 -> 2; matrix products, arithmetic and copies ran while one was open for 0% -> 0% of each run, Pallas kernels for 1% -> 1%
where the time goes in v3:
time: 94.7 us; the launch traced here: 94.2 us
  blocking collectives  54.6 us (58%)
  starting transfers between devices  21.2 us (22%)
  waiting for transfers between devices  9.12 us (10%)
  Pallas kernels  8.59 us (9%)
    all_gather x6, blocking collectives, gather_pairs(): x = lax.all_gather(x, axis, axis=0)  32.7 us
    all_to_all x2, blocking collectives, exchange(): lax.all_to_all(x, axes, split_axis=0, concat_axis=0, tiled=True)  21.9 us
    all_to_all x2, starting transfers between devices, exchange(): lax.all_to_all(x, axes, split_axis=0, concat_axis=0, tiled=True)  21.2 us
    all_to_all x2, waiting for transfers between devices, exchange(): lax.all_to_all(x, axes, split_axis=0, concat_axis=0, tiled=True)  9.12 us
    pallas_call x6, Pallas kernels, call(): pl.pallas_call(body, out_shape=shapes, scratch_shapes=list(scratch), name...  8.59 us
  transfers between devices with their start and end apart: 2, of which 2 were waited for; matrix products, arithmetic and copies ran while one was open for 0% of the time, Pallas kernels for 1%

profile of v3, /device:TPU:6, one launch (start us, length us, event | category | flops | bytes accessed | tf_op | source)
XLA Modules:
  0.0 94.2 jit_solution(706774132104676058)
XLA Ops:
  0.6 1.6 %prepare_queries.1 = bf16[8,176,128]{2,1,0:T(8,128)(2,1)} custom-call(bf16[96,128]{1,0:T(8,128)(2,1)} %bitcast.21, f32[1,128]{1,0:T(1,128)} %bitcast.25, bf16[64,128]{1,0:T(8,128)(2,1)} %bitcast.22, bf16[64,128]{1,0:T(8,128)(2,1)} %bitcast.23), custom_call_target="tpu_custom_call" | custom-call | tf_op jit(solution)/shard_map/prepare_queries/pallas_call | solution.py:145
  2.2 15.1 %all-to-all-start = ((bf16[8,176,128]{2,1,0:T(8,128)(2,1)}), bf16[8,176,128]{2,1,0:T(8,128)(2,1)S(1)}, u32[]{:S(2)}, u32[]{:S(2)}) async-start(bf16[8,176,128]{2,1,0:T(8,128)(2,1)} %prepare_queries.1), calls=%async_computation | async-start | bytes 720896 | tf_op jit(solution)/shard_map/all_to_all | solution.py:153
  17.3 1.2 %prepare_keys.1 = bf16[160,128]{1,0:T(8,128)(2,1)S(1)} custom-call(bf16[128,512]{1,0:T(8,128)(2,1)} %latents.3, bf16[32,128]{1,0:T(8,128)(2,1)} %bitcast.24, bf16[512,128]{1,0:T(8,128)(2,1)} %weight.1), custom_call_target="tpu_custom_call" | custom-call | tf_op jit(solution)/shard_map/prepare_keys/pallas_call | solution.py:145
  18.5 4.7 %all-gather = bf16[320,128]{1,0:T(8,128)(2,1)S(1)} all-gather(bf16[160,128]{1,0:T(8,128)(2,1)S(1)} %prepare_keys.1), channel_id=2, replica_groups=mesh['z3'=2,'z2'=2,'z1'=2,'z0'=2,'y1'=2,'y0'=2,'x1'=2,'x0'=2,'c'=2] {'y0'}, dimensions={0}, use_global_device_ids=true | all-gather | bytes 122880 | tf_op jit(solution)/shard_map/all_gather | solution.py:158
  23.2 6.6 %all-gather.1 = bf16[4,160,128]{2,1,0:T(8,128)(2,1)S(1)} all-gather(bf16[2,160,128]{2,1,0:T(8,128)(2,1)S(1)} %bitcast.18), channel_id=3, replica_groups=mesh['z3'=2,'z2'=2,'z1'=2,'z0'=2,'y1'=2,'y0'=2,'x1'=2,'x0'=2,'c'=2] {'y1'}, dimensions={0}, use_global_device_ids=true | all-gather | bytes 245760 | tf_op jit(solution)/shard_map/all_gather | solution.py:158
  29.8 8.6 %all-gather.2 = bf16[4,2,160,128]{3,2,1,0:T(8,128)(2,1)S(1)} all-gather(bf16[2,2,160,128]{3,2,1,0:T(8,128)(2,1)S(1)} %bitcast.17), channel_id=4, replica_groups=mesh['z3'=2,'z2'=2,'z1'=2,'z0'=2,'y1'=2,'y0'=2,'x1'=2,'x0'=2,'c'=2] {'z0'}, dimensions={0}, use_global_device_ids=true | all-gather | bytes 491520 | tf_op jit(solution)/shard_map/all_gather | solution.py:158
  38.4 4.4 %all-to-all-done.q_all = bf16[8,176,128]{2,1,0:T(8,128)(2,1)S(1)} async-done(((bf16[8,176,128]{2,1,0:T(8,128)(2,1)}), bf16[8,176,128]{2,1,0:T(8,128)(2,1)S(1)}, u32[]{:S(2)}, u32[]{:S(2)}) %all-to-all-start) | async-done | bytes 360480 | tf_op jit(solution)/shard_map/all_to_all | solution.py:153
  42.8 2.9 %attend.1 = (bf16[8,96,128]{2,1,0:T(8,128)(2,1)S(1)}, bf16[8,160,128]{2,1,0:T(8,128)(2,1)S(1)}) custom-call(bf16[8,176,128]{2,1,0:T(8,128)(2,1)S(1)} %all-to-all-done.q_all, bf16[8,160,128]{2,1,0:T(8,128)(2,1)S(1)} %bitcast.15), custom_call_target="tpu_custom_call" | custom-call | tf_op jit(solution)/shard_map/attend/pallas_call | solution.py:145
  45.7 12.9 %all_to_all.20.dkv = bf16[8,160,128]{2,1,0:T(8,128)(2,1)S(1)} all-to-all(bf16[8,160,128]{2,1,0:T(8,128)(2,1)S(1)} %get-tuple-element.14), channel_id=1, replica_groups=mesh['z3'=2,'z2'=2,'z1'=2,'z0'=2,'y1'=2,'y0'=2,'x1'=2,'x0'=2,'c'=2] {'z0..., dimensions={0} | all-to-all | bytes 655360 | tf_op jit(solution)/shard_map/all_to_all | solution.py:153
  58.7 1.6 %finish_keys.1 = (bf16[64,128]{1,0:T(8,128)(2,1)}, bf16[64,128]{1,0:T(8,128)(2,1)}, f32[32,128]{1,0:T(8,128)S(1)}, bf16[8,64,128]{2,1,0:T(8,128)(2,1)S(1)}) custom-call(bf16[8,160,128]{2,1,0:T(8,128)(2,1)S(1)} %all_to_all.20.dkv, bf16[128,512]{1,0:T(8,128)(2,1)} %latents.3), custom_call_target="tpu_custom_call" | custom-call | tf_op jit(solution)/shard_map/finish_keys/pallas_call | solution.py:145
  60.2 9.0 %all_to_all.21.weight = bf16[8,64,128]{2,1,0:T(8,128)(2,1)S(1)} all-to-all(bf16[8,64,128]{2,1,0:T(8,128)(2,1)S(1)} %get-tuple-element.15), channel_id=1, replica_groups=mesh['z3'=2,'z2'=2,'z1'=2,'z0'=2,'y1'=2,'y0'=2,'x1'=2,'x0'=2,'c'=2] {'z0..., dimensions={0} | all-to-all | bytes 262144 | tf_op jit(solution)/shard_map/all_to_all | solution.py:153
  69.2 0.7 join_far.1
  69.9 6.1 %all-to-all-start.3 = ((bf16[8,112,128]{2,1,0:T(8,128)(2,1)}), bf16[8,112,128]{2,1,0:T(8,128)(2,1)S(1)}, u32[]{:S(2)}, u32[]{:S(2)}) async-start(bf16[8,112,128]{2,1,0:T(8,128)(2,1)} %join_far.1), calls=%async_computation.3 | async-start | bytes 458752 | tf_op jit(solution)/shard_map/all_to_all | solution.py:153
  76.0 1.8 %all-gather.3 = f32[64,128]{1,0:T(8,128)S(1)} all-gather(f32[32,128]{1,0:T(8,128)S(1)} %get-tuple-element.17), channel_id=5, replica_groups=mesh['z3'=2,'z2'=2,'z1'=2,'z0'=2,'y1'=2,'y0'=2,'x1'=2,'x0'=2,'c'=2] {'c'}, dimensions={0}, use_global_device_ids=true | all-gather | bytes 49152 | tf_op jit(solution)/shard_map/all_gather | solution.py:158
  77.8 4.6 %all-gather.4 = f32[4,32,128]{2,1,0:T(8,128)S(1)} all-gather(f32[2,32,128]{2,1,0:T(8,128)S(1)} %bitcast.20), channel_id=6, replica_groups=mesh['z3'=2,'z2'=2,'z1'=2,'z0'=2,'y1'=2,'y0'=2,'x1'=2,'x0'=2,'c'=2] {'x0'}, dimensions={0}, use_global_device_ids=true | all-gather | bytes 98304 | tf_op jit(solution)/shard_map/all_gather | solution.py:158
  82.4 6.4 %all-gather.5 = f32[4,2,32,128]{3,2,1,0:T(8,128)S(1)} all-gather(f32[2,2,32,128]{3,2,1,0:T(8,128)S(1)} %bitcast.19), channel_id=7, replica_groups=mesh['z3'=2,'z2'=2,'z1'=2,'z0'=2,'y1'=2,'y0'=2,'x1'=2,'x0'=2,'c'=2] {'x1'}, dimensions={0}, use_global_device_ids=true | all-gather | bytes 196608 | tf_op jit(solution)/shard_map/all_gather | solution.py:158
  88.8 4.7 %all-to-all-done.3.far = bf16[8,112,128]{2,1,0:T(8,128)(2,1)S(1)} async-done(((bf16[8,112,128]{2,1,0:T(8,128)(2,1)}), bf16[8,112,128]{2,1,0:T(8,128)(2,1)S(1)}, u32[]{:S(2)}, u32[]{:S(2)}) %all-to-all-start.3) | async-done | bytes 229408 | tf_op jit(solution)/shard_map/all_to_all | solution.py:153
  93.5 0.6 finish_rest.1
Async XLA Ops:
  2.2 40.7 %all-to-all-start = ((bf16[8,176,128]{2,1,0:T(8,128)(2,1)}), bf16[8,176,128]{2,1,0:T(8,128)(2,1)S(1)}, u32[]{:S(2)}, u32[]{:S(2)}) async-start(bf16[8,176,128]{2,1,0:T(8,128)(2,1)} %prepare_queries.1), calls=%async_computation | async-start | bytes 720896 | tf_op jit(solution)/shard_map/all_to_all | solution.py:153
  69.9 23.6 %all-to-all-start.3 = ((bf16[8,112,128]{2,1,0:T(8,128)(2,1)}), bf16[8,112,128]{2,1,0:T(8,128)(2,1)S(1)}, u32[]{:S(2)}, u32[]{:S(2)}) async-start(bf16[8,112,128]{2,1,0:T(8,128)(2,1)} %join_far.1), calls=%async_computation.3 | async-start | bytes 458752 | tf_op jit(solution)/shard_map/all_to_all | solution.py:153

commit v4 on v3

--- a/solution.py
+++ b/solution.py
@@ -33,22 +33,17 @@
     return high.astype(F32), middle.astype(F32), low.astype(F32)
 
 
-def prepare_keys(latents, rot_key, weight, k_out):
+def prepare(latents, rot_key, weight, queries, logs, outputs, grads, k_out, q_out):
     joined = lax.dot_general(
         latents[...], weight[...], (((1,), (0,)), ((), ())), preferred_element_type=F32
     )
     joined_t = joined.T.astype(BF)
-    block = jnp.concatenate(
-        [joined_t[:NOPE_DIM], rot_key[...], joined_t[NOPE_DIM:]], axis=0
-    )
-    k_out[...] = block
-
-
-def prepare_queries(queries, logs, outputs, grads, q_out):
+    k_out[:NOPE_DIM] = joined_t[:NOPE_DIM]
+    k_out[NOPE_DIM:HEAD_DIM] = rot_key[...]
+    k_out[HEAD_DIM:] = joined_t[NOPE_DIM:]
     q_t = queries[...].astype(F32)
     g_t = grads[...].astype(F32)
-    o_t = outputs[...].astype(F32)
-    delta = jnp.sum(o_t * g_t, axis=0, keepdims=True)
+    delta = jnp.sum(outputs[...].astype(F32) * g_t, axis=0, keepdims=True)
     rows = three_parts(logs[...] * (-1.0 / SCALE)) + three_parts(-delta)
     index = lax.broadcasted_iota(jnp.int32, (PAD, TOK), 0)
     pad = jnp.zeros((PAD, TOK), F32)
@@ -71,7 +66,7 @@
         tok = q_block.astype(F32).T
         q_tok[at, :] = tok[:, :HEAD_DIM].astype(BF)
         g_tok[at, :] = tok[:, HEAD_DIM + PAD :].astype(BF)
-        k_block = k_all[i]
+        k_block = k_all[(i % 4) * 2 + i // 4]
         k_t[:, at] = k_block[:HEAD_DIM]
         ktok = k_block.astype(F32).T
         k_tok[at, :] = jnp.concatenate([ktok[:, :HEAD_DIM], key_pad], axis=1).astype(BF)
@@ -156,25 +151,21 @@
 def gather_pairs(x, axes):
     for axis in axes:
         x = lax.all_gather(x, axis, axis=0)
-    return close(x.reshape((GROUP,) + x.shape[len(axes) :]))
+    return x
 
 
 def per_device(queries, latents, rot_key, kv_weight, log_sums, outputs, out_grad):
     total = GROUP * TOK
-    (k_send,) = call(
-        prepare_keys,
-        (latents, rot_key.T, kv_weight),
-        [((K_ROWS, TOK), BF, True)],
-        "prepare_keys",
-    )
-    (q_send,) = call(
-        prepare_queries,
-        (queries.T, log_sums.T, outputs.T, out_grad.T),
-        [((GROUP, Q_ROWS, TOK), BF, True)],
-        "prepare_queries",
-    )
-    k_all = gather_pairs(k_send, NEAR[::-1])
+    k_send, q_send = call(
+        prepare,
+        (latents, rot_key.T, kv_weight, queries.T, log_sums.T, outputs.T, out_grad.T),
+        [((K_ROWS, TOK), BF, True), ((GROUP, Q_ROWS, TOK), BF, False)],
+        "prepare",
+    )
+    k_pair = gather_pairs(k_send, ("z0",))
+    q_send, k_pair = lax.optimization_barrier((q_send, k_pair))
     q_all = exchange(q_send, FAR)
+    k_all = close(gather_pairs(k_pair, ("y0", "y1")).reshape(GROUP, K_ROWS, TOK))
     dq, dkv = call(
         attend,
         (q_all, k_all),
@@ -205,7 +196,7 @@
         ],
         "finish_keys",
     )
-    rot_all = gather_pairs(rot_send, HEADS_AXIS[::-1])
+    rot_all = close(gather_pairs(rot_send, HEADS_AXIS[::-1]).reshape(GROUP, ROPE_DIM, TOK))
     (far_send,) = call(
         join_far,
         (exchange(weight_send, NEAR), close(dq)),

time: 94.7 us -> 95.5 us (level)
  waiting for transfers between devices: 9.12 us -> 15.4 us
  blocking collectives: 54.6 us -> 51.9 us
  starting transfers between devices: 21.2 us -> 19.3 us
    all_to_all x2, waiting for transfers between devices: 9.12 us -> 15.4 us  [exchange(): lax.all_to_all(x, axes, split_axis=0, concat_axis=0, tiled=True)]
    all_gather x6, blocking collectives: 32.7 us -> 30 us  [gather_pairs(): x = lax.all_gather(x, axis, axis=0)]
    all_to_all x2, starting transfers between devices: 21.2 us -> 19.3 us  [exchange(): lax.all_to_all(x, axes, split_axis=0, concat_axis=0, tiled=True)]
    pallas_call x6 -> x5, Pallas kernels: 8.59 us -> 7.78 us  [call(): pl.pallas_call(body, out_shape=shapes, scratch_shapes=list(scratch), name...]
  transfers between devices with their start and end apart: 2 -> 2, of which waited for: 2 -> 2; matrix products, arithmetic and copies ran while one was open for 0% -> 0% of each run, Pallas kernels for 1% -> 0%
where the time goes in v4:
time: 95.5 us; the launch traced here: 95 us
  blocking collectives  51.9 us (54%)
  starting transfers between devices  19.3 us (20%)
  waiting for transfers between devices  15.4 us (16%)
  Pallas kernels  7.78 us (8%)
    all_gather x6, blocking collectives, gather_pairs(): x = lax.all_gather(x, axis, axis=0)  30 us
    all_to_all x2, blocking collectives, exchange(): lax.all_to_all(x, axes, split_axis=0, concat_axis=0, tiled=True)  21.9 us
    all_to_all x2, starting transfers between devices, exchange(): lax.all_to_all(x, axes, split_axis=0, concat_axis=0, tiled=True)  19.3 us
    all_to_all x2, waiting for transfers between devices, exchange(): lax.all_to_all(x, axes, split_axis=0, concat_axis=0, tiled=True)  15.4 us
    pallas_call x5, Pallas kernels, call(): pl.pallas_call(body, out_shape=shapes, scratch_shapes=list(scratch), name...  7.78 us
  transfers between devices with their start and end apart: 2, of which 2 were waited for; matrix products, arithmetic and copies ran while one was open for 0% of the time, Pallas kernels for 0%

profile of v4, /device:TPU:6, one launch (start us, length us, event | category | flops | bytes accessed | tf_op | source)
XLA Modules:
  0.0 95.0 jit_solution(7901212881081007770)
XLA Ops:
  0.6 2.0 %prepare.1 = (bf16[160,128]{1,0:T(8,128)(2,1)S(1)}, bf16[8,176,128]{2,1,0:T(8,128)(2,1)}) custom-call(bf16[128,512]{1,0:T(8,128)(2,1)} %latents.3, bf16[32,128]{1,0:T(8,128)(2,1)} %bitcast.24, bf16[512,128]{1,0:T(8,128)(2,1)} %weight.1, bf16[96,128]{1,0:T(8,128)(2,1)} %bitcast.21, f32[1,128]{1,0:T(1,128)} %bitcast.25, bf16[64,128]{1,0:T(8,128)(2,1)} %bitcast.22, ...), custom_call_target="tpu_custom_call" | custom-call | tf_op jit(solution)/shard_map/prepare/pallas_call | solution.py:140
  2.6 4.7 %all-gather = bf16[320,128]{1,0:T(8,128)(2,1)S(1)} all-gather(bf16[160,128]{1,0:T(8,128)(2,1)S(1)} %get-tuple-element.19), channel_id=2, replica_groups=mesh['z3'=2,'z2'=2,'z1'=2,'z0'=2,'y1'=2,'y0'=2,'x1'=2,'x0'=2,'c'=2] {'z0'}, dimensions={0}, use_global_device_ids=true | all-gather | bytes 122880 | tf_op jit(solution)/shard_map/all_gather | solution.py:153
  7.3 15.1 %all-to-all-start = ((bf16[8,176,128]{2,1,0:T(8,128)(2,1)}), bf16[8,176,128]{2,1,0:T(8,128)(2,1)S(1)}, u32[]{:S(2)}, u32[]{:S(2)}) async-start(bf16[8,176,128]{2,1,0:T(8,128)(2,1)} %get-tuple-element.20), calls=%async_computation | async-start | bytes 720896 | tf_op jit(solution)/shard_map/all_to_all | solution.py:148
  22.3 5.1 %all-gather.1 = bf16[4,160,128]{2,1,0:T(8,128)(2,1)S(1)} all-gather(bf16[2,160,128]{2,1,0:T(8,128)(2,1)S(1)} %bitcast.18), channel_id=3, replica_groups=mesh['z3'=2,'z2'=2,'z1'=2,'z0'=2,'y1'=2,'y0'=2,'x1'=2,'x0'=2,'c'=2] {'y0'}, dimensions={0}, use_global_device_ids=true | all-gather | bytes 245760 | tf_op jit(solution)/shard_map/all_gather | solution.py:153
  27.4 7.5 %all-gather.2 = bf16[4,2,160,128]{3,2,1,0:T(8,128)(2,1)S(1)} all-gather(bf16[2,2,160,128]{3,2,1,0:T(8,128)(2,1)S(1)} %bitcast.17), channel_id=4, replica_groups=mesh['z3'=2,'z2'=2,'z1'=2,'z0'=2,'y1'=2,'y0'=2,'x1'=2,'x0'=2,'c'=2] {'y1'}, dimensions={0}, use_global_device_ids=true | all-gather | bytes 491520 | tf_op jit(solution)/shard_map/all_gather | solution.py:153
  34.9 10.6 %all-to-all-done.q_all = bf16[8,176,128]{2,1,0:T(8,128)(2,1)S(1)} async-done(((bf16[8,176,128]{2,1,0:T(8,128)(2,1)}), bf16[8,176,128]{2,1,0:T(8,128)(2,1)S(1)}, u32[]{:S(2)}, u32[]{:S(2)}) %all-to-all-start) | async-done | bytes 360480 | tf_op jit(solution)/shard_map/all_to_all | solution.py:148
  45.5 2.9 %attend.1 = (bf16[8,96,128]{2,1,0:T(8,128)(2,1)S(1)}, bf16[8,160,128]{2,1,0:T(8,128)(2,1)S(1)}) custom-call(bf16[8,176,128]{2,1,0:T(8,128)(2,1)S(1)} %all-to-all-done.q_all, bf16[8,160,128]{2,1,0:T(8,128)(2,1)S(1)} %bitcast.15), custom_call_target="tpu_custom_call" | custom-call | tf_op jit(solution)/shard_map/attend/pallas_call | solution.py:140
  48.4 12.7 %all_to_all.20.dkv = bf16[8,160,128]{2,1,0:T(8,128)(2,1)S(1)} all-to-all(bf16[8,160,128]{2,1,0:T(8,128)(2,1)S(1)} %get-tuple-element.22), channel_id=1, replica_groups=mesh['z3'=2,'z2'=2,'z1'=2,'z0'=2,'y1'=2,'y0'=2,'x1'=2,'x0'=2,'c'=2] {'z0..., dimensions={0} | all-to-all | bytes 655360 | tf_op jit(solution)/shard_map/all_to_all | solution.py:148
  61.1 1.6 %finish_keys.1 = (bf16[64,128]{1,0:T(8,128)(2,1)}, bf16[64,128]{1,0:T(8,128)(2,1)}, f32[32,128]{1,0:T(8,128)S(1)}, bf16[8,64,128]{2,1,0:T(8,128)(2,1)S(1)}) custom-call(bf16[8,160,128]{2,1,0:T(8,128)(2,1)S(1)} %all_to_all.20.dkv, bf16[128,512]{1,0:T(8,128)(2,1)} %latents.3), custom_call_target="tpu_custom_call" | custom-call | tf_op jit(solution)/shard_map/finish_keys/pallas_call | solution.py:140
  62.6 9.2 %all_to_all.21.weight = bf16[8,64,128]{2,1,0:T(8,128)(2,1)S(1)} all-to-all(bf16[8,64,128]{2,1,0:T(8,128)(2,1)S(1)} %get-tuple-element.23), channel_id=1, replica_groups=mesh['z3'=2,'z2'=2,'z1'=2,'z0'=2,'y1'=2,'y0'=2,'x1'=2,'x0'=2,'c'=2] {'z0..., dimensions={0} | all-to-all | bytes 262144 | tf_op jit(solution)/shard_map/all_to_all | solution.py:148
  71.8 0.7 join_far.1
  72.5 4.2 %all-to-all-start.3 = ((bf16[8,112,128]{2,1,0:T(8,128)(2,1)}), bf16[8,112,128]{2,1,0:T(8,128)(2,1)S(1)}, u32[]{:S(2)}, u32[]{:S(2)}) async-start(bf16[8,112,128]{2,1,0:T(8,128)(2,1)} %join_far.1), calls=%async_computation.3 | async-start | bytes 458752 | tf_op jit(solution)/shard_map/all_to_all | solution.py:148
  76.7 1.8 %all-gather.3 = f32[64,128]{1,0:T(8,128)S(1)} all-gather(f32[32,128]{1,0:T(8,128)S(1)} %get-tuple-element.25), channel_id=5, replica_groups=mesh['z3'=2,'z2'=2,'z1'=2,'z0'=2,'y1'=2,'y0'=2,'x1'=2,'x0'=2,'c'=2] {'c'}, dimensions={0}, use_global_device_ids=true | all-gather | bytes 49152 | tf_op jit(solution)/shard_map/all_gather | solution.py:153
  78.5 4.6 %all-gather.4 = f32[4,32,128]{2,1,0:T(8,128)S(1)} all-gather(f32[2,32,128]{2,1,0:T(8,128)S(1)} %bitcast.20), channel_id=6, replica_groups=mesh['z3'=2,'z2'=2,'z1'=2,'z0'=2,'y1'=2,'y0'=2,'x1'=2,'x0'=2,'c'=2] {'x0'}, dimensions={0}, use_global_device_ids=true | all-gather | bytes 98304 | tf_op jit(solution)/shard_map/all_gather | solution.py:153
  83.1 6.4 %all-gather.5 = f32[4,2,32,128]{3,2,1,0:T(8,128)S(1)} all-gather(f32[2,2,32,128]{3,2,1,0:T(8,128)S(1)} %bitcast.19), channel_id=7, replica_groups=mesh['z3'=2,'z2'=2,'z1'=2,'z0'=2,'y1'=2,'y0'=2,'x1'=2,'x0'=2,'c'=2] {'x1'}, dimensions={0}, use_global_device_ids=true | all-gather | bytes 196608 | tf_op jit(solution)/shard_map/all_gather | solution.py:153
  89.5 4.9 %all-to-all-done.3.far = bf16[8,112,128]{2,1,0:T(8,128)(2,1)S(1)} async-done(((bf16[8,112,128]{2,1,0:T(8,128)(2,1)}), bf16[8,112,128]{2,1,0:T(8,128)(2,1)S(1)}, u32[]{:S(2)}, u32[]{:S(2)}) %all-to-all-start.3) | async-done | bytes 229408 | tf_op jit(solution)/shard_map/all_to_all | solution.py:148
  94.4 0.6 finish_rest.1
Async XLA Ops:
  7.3 38.2 %all-to-all-start = ((bf16[8,176,128]{2,1,0:T(8,128)(2,1)}), bf16[8,176,128]{2,1,0:T(8,128)(2,1)S(1)}, u32[]{:S(2)}, u32[]{:S(2)}) async-start(bf16[8,176,128]{2,1,0:T(8,128)(2,1)} %get-tuple-element.20), calls=%async_computation | async-start | bytes 720896 | tf_op jit(solution)/shard_map/all_to_all | solution.py:148
  72.5 21.9 %all-to-all-start.3 = ((bf16[8,112,128]{2,1,0:T(8,128)(2,1)}), bf16[8,112,128]{2,1,0:T(8,128)(2,1)S(1)}, u32[]{:S(2)}, u32[]{:S(2)}) async-start(bf16[8,112,128]{2,1,0:T(8,128)(2,1)} %join_far.1), calls=%async_computation.3 | async-start | bytes 458752 | tf_op jit(solution)/shard_map/all_to_all | solution.py:148

commit v5 on v4

--- a/solution.py
+++ b/solution.py
@@ -12,7 +12,8 @@
 VALUE_DIM = 64
 HEAD_DIM = NOPE_DIM + ROPE_DIM
 SCALE = HEAD_DIM**-0.5
-PAD = 16
+PAD = 8
+FAR_ROWS = HEAD_DIM + 8
 Q_ROWS = HEAD_DIM + PAD + VALUE_DIM
 K_ROWS = HEAD_DIM + VALUE_DIM
 BF = jnp.bfloat16
@@ -33,7 +34,8 @@
     return high.astype(F32), middle.astype(F32), low.astype(F32)
 
 
-def prepare(latents, rot_key, weight, queries, logs, outputs, grads, k_out, q_out):
+def prepare(latents, rot_key, weight, queries, logs, outputs, grads, k_out, q_out, latents_out):
+    latents_out[...] = latents[...]
     joined = lax.dot_general(
         latents[...], weight[...], (((1,), (0,)), ((), ())), preferred_element_type=F32
     )
@@ -54,7 +56,7 @@
         q_out[i] = block
 
 
-def attend(q_all, k_all, dq_out, dkv_out, q_t, q_tok, g_tok, k_t, k_tok, v_tok, dq_acc, dk_acc, dv_acc, dscores, probs_b):
+def attend(q_all, k_all, far_out, dkv_out, q_t, q_tok, g_tok, k_t, k_tok, v_tok, dq_acc, dk_acc, dv_acc, dscores, probs_b, far_block, sem):
     total = GROUP * TOK
     lane = lax.broadcasted_iota(jnp.int32, (TOK, PAD), 1)
     key_pad = jnp.where(lane < 3, 1.0, 0.0).astype(F32)
@@ -66,7 +68,7 @@
         tok = q_block.astype(F32).T
         q_tok[at, :] = tok[:, :HEAD_DIM].astype(BF)
         g_tok[at, :] = tok[:, HEAD_DIM + PAD :].astype(BF)
-        k_block = k_all[(i % 4) * 2 + i // 4]
+        k_block = k_all[i]
         k_t[:, at] = k_block[:HEAD_DIM]
         ktok = k_block.astype(F32).T
         k_tok[at, :] = jnp.concatenate([ktok[:, :HEAD_DIM], key_pad], axis=1).astype(BF)
@@ -87,11 +89,16 @@
         qs = slice(qi * step, (qi + 1) * step)
         dq_acc[:, qs] = jnp.dot(k_t[...], dscores[:, qs], preferred_element_type=F32)
     for i in range(GROUP):
+        far_block[i, :HEAD_DIM] = (dq_acc[:, i * TOK : (i + 1) * TOK] * SCALE).astype(BF)
+        far_block[i, HEAD_DIM:] = jnp.zeros((8, TOK), BF)
+    copy = pltpu.make_async_copy(far_block, far_out, sem)
+    copy.start()
+    for i in range(GROUP):
         at = slice(i * TOK, (i + 1) * TOK)
-        dq_out[i] = (dq_acc[:, at] * SCALE).astype(BF)
         dkv_out[i] = jnp.concatenate(
             [(dk_acc[at, :] * SCALE).T, dv_acc[at, :].T], axis=0
         ).astype(BF)
+    copy.wait()
 
 
 def finish_keys(dkv, latents, key_grad, value_grad, rot_out, weight_out):
@@ -110,15 +117,15 @@
         weight_out[i] = by_owner[:, i].reshape(GROUP * 8, TOK).astype(BF)
 
 
-def join_far(weight, dq, far_out):
+def join_far(weight, far_in, far_out, rows, sem):
+    del far_in
     total = weight[0].astype(F32)
     for i in range(1, GROUP):
         total = total + weight[i].astype(F32)
-    for i in range(GROUP):
-        rows = total[i * 8 : (i + 1) * 8]
-        high = rows.astype(BF).astype(F32)
-        far_out[i, :HEAD_DIM] = dq[i]
-        far_out[i, HEAD_DIM:] = jnp.concatenate([high, rows - high], axis=0).astype(BF)
+    rows[...] = total.reshape(GROUP, 8, TOK).astype(BF)
+    copy = pltpu.make_async_copy(rows, far_out.at[:, HEAD_DIM:], sem)
+    copy.start()
+    copy.wait()
 
 
 def finish_rest(far, rot, query_grad, weight_grad, rot_grad):
@@ -128,16 +135,18 @@
         total = total + far[i].astype(F32)
         around = around + rot[i]
     query_grad[...] = total[:HEAD_DIM].astype(BF)
-    weight_grad[...] = total[HEAD_DIM : HEAD_DIM + 8] + total[HEAD_DIM + 8 :]
+    weight_grad[...] = total[HEAD_DIM:]
     rot_grad[...] = around
 
 
-def call(body, args, outs, name, scratch=()):
+def call(body, args, outs, name, scratch=(), **more):
     shapes = [
         pltpu.VMEM(shape, kind) if near else jax.ShapeDtypeStruct(shape, kind)
         for shape, kind, near in outs
     ]
-    return pl.pallas_call(body, out_shape=shapes, scratch_shapes=list(scratch), name=name)(*args)
+    return pl.pallas_call(body, out_shape=shapes, scratch_shapes=list(scratch), name=name, **more)(
+        *args
+    )
 
 
 def close(x):
@@ -156,20 +165,18 @@
 
 def per_device(queries, latents, rot_key, kv_weight, log_sums, outputs, out_grad):
     total = GROUP * TOK
-    k_send, q_send = call(
+    k_send, q_send, latents_kept = call(
         prepare,
         (latents, rot_key.T, kv_weight, queries.T, log_sums.T, outputs.T, out_grad.T),
-        [((K_ROWS, TOK), BF, True), ((GROUP, Q_ROWS, TOK), BF, False)],
+        [((K_ROWS, TOK), BF, True), ((GROUP, Q_ROWS, TOK), BF, False), (latents.shape, BF, True)],
         "prepare",
     )
-    k_pair = gather_pairs(k_send, ("z0",))
-    q_send, k_pair = lax.optimization_barrier((q_send, k_pair))
     q_all = exchange(q_send, FAR)
-    k_all = close(gather_pairs(k_pair, ("y0", "y1")).reshape(GROUP, K_ROWS, TOK))
-    dq, dkv = call(
+    k_all = close(gather_pairs(k_send, NEAR[::-1]).reshape(GROUP, K_ROWS, TOK))
+    far_send, dkv = call(
         attend,
         (q_all, k_all),
-        [((GROUP, HEAD_DIM, TOK), BF, True), ((GROUP, K_ROWS, TOK), BF, True)],
+        [((GROUP, FAR_ROWS, TOK), BF, False), ((GROUP, K_ROWS, TOK), BF, True)],
         "attend",
         [
             pltpu.VMEM((Q_ROWS, total), BF),
@@ -183,11 +190,14 @@
             pltpu.VMEM((total, VALUE_DIM), F32),
             pltpu.VMEM((total, total), BF),
             pltpu.VMEM((total, total), BF),
+            pltpu.VMEM((GROUP, FAR_ROWS, TOK), BF),
+            pltpu.SemaphoreType.DMA,
         ],
+        out_specs=[pl.BlockSpec(memory_space=pl.ANY), pl.BlockSpec(memory_space=pltpu.VMEM)],
     )
     key_grad, value_grad, rot_send, weight_send = call(
         finish_keys,
-        (exchange(dkv, NEAR), latents),
+        (exchange(dkv, NEAR), close(latents_kept)),
         [
             ((NOPE_DIM, TOK), BF, False),
             ((VALUE_DIM, TOK), BF, False),
@@ -199,9 +209,13 @@
     rot_all = close(gather_pairs(rot_send, HEADS_AXIS[::-1]).reshape(GROUP, ROPE_DIM, TOK))
     (far_send,) = call(
         join_far,
-        (exchange(weight_send, NEAR), close(dq)),
-        [((GROUP, HEAD_DIM + 16, TOK), BF, True)],
+        (exchange(weight_send, NEAR), far_send),
+        [((GROUP, FAR_ROWS, TOK), BF, False)],
         "join_far",
+        [pltpu.VMEM((GROUP, 8, TOK), BF), pltpu.SemaphoreType.DMA],
+        in_specs=[pl.BlockSpec(memory_space=pltpu.VMEM), pl.BlockSpec(memory_space=pl.ANY)],
+        out_specs=[pl.BlockSpec(memory_space=pl.ANY)],
+        input_output_aliases={1: 0},
     )
     query_grad, weight_grad, rot_grad = call(
         finish_rest,

time: 95.5 us -> 93.8 us (0.982)
  waiting for transfers between devices: 15.4 us -> 9.34 us
  blocking collectives: 51.9 us -> 54.7 us
  starting transfers between devices: 19.3 us -> 21.2 us
    all_to_all x2, waiting for transfers between devices: 15.4 us -> 9.34 us  [exchange(): lax.all_to_all(x, axes, split_axis=0, concat_axis=0, tiled=True)]
    all_gather x6, blocking collectives: 30 us -> 32.7 us  [gather_pairs(): x = lax.all_gather(x, axis, axis=0)]
    all_to_all x2, starting transfers between devices: 19.3 us -> 21.2 us  [exchange(): lax.all_to_all(x, axes, split_axis=0, concat_axis=0, tiled=True)]
where the time goes in v5:
time: 93.8 us; the launch traced here: 93.4 us
  blocking collectives  54.7 us (58%)
  starting transfers between devices  21.2 us (23%)
  waiting for transfers between devices  9.34 us (10%)
  Pallas kernels  7.47 us (8%)
    all_gather x6, blocking collectives, gather_pairs(): x = lax.all_gather(x, axis, axis=0)  32.7 us
    all_to_all x2, blocking collectives, exchange(): lax.all_to_all(x, axes, split_axis=0, concat_axis=0, tiled=True)  22 us
    all_to_all x2, starting transfers between devices, exchange(): lax.all_to_all(x, axes, split_axis=0, concat_axis=0, tiled=True)  21.2 us
    all_to_all x2, waiting for transfers between devices, exchange(): lax.all_to_all(x, axes, split_axis=0, concat_axis=0, tiled=True)  9.34 us
    pallas_call x5, Pallas kernels, call(): pl.pallas_call(body, out_shape=shapes, scratch_shapes=list(scratch), name...  7.47 us
  transfers between devices with their start and end apart: 2, of which 2 were waited for; matrix products, arithmetic and copies ran while one was open for 0% of the time, Pallas kernels for 0%

profile of v5, /device:TPU:6, one launch (start us, length us, event | category | flops | bytes accessed | tf_op | source)
XLA Modules:
  0.0 93.4 jit_solution(8101934770378353058)
XLA Ops:
  0.6 2.0 %prepare.1 = (bf16[160,128]{1,0:T(8,128)(2,1)S(1)}, bf16[8,168,128]{2,1,0:T(8,128)(2,1)}, bf16[128,512]{1,0:T(8,128)(2,1)S(1)}) custom-call(bf16[128,512]{1,0:T(8,128)(2,1)} %latents.1, bf16[32,128]{1,0:T(8,128)(2,1)} %bitcast.24, bf16[512,128]{1,0:T(8,128)(2,1)} %weight.1, bf16[96,128]{1,0:T(8,128)(2,1)} %bitcast.21, f32[1,128]{1,0:T(1,128)} %bitcast.25, ...), custom_call_target="tpu_custom_call" | custom-call | tf_op jit(solution)/shard_map/prepare/pallas_call | solution.py:147
  2.6 15.1 %all-to-all-start = ((bf16[8,168,128]{2,1,0:T(8,128)(2,1)}), bf16[8,168,128]{2,1,0:T(8,128)(2,1)S(1)}, u32[]{:S(2)}, u32[]{:S(2)}) async-start(bf16[8,168,128]{2,1,0:T(8,128)(2,1)} %get-tuple-element.17), calls=%async_computation | async-start | bytes 688128 | tf_op jit(solution)/shard_map/all_to_all | solution.py:157
  17.7 4.7 %all-gather = bf16[320,128]{1,0:T(8,128)(2,1)S(1)} all-gather(bf16[160,128]{1,0:T(8,128)(2,1)S(1)} %get-tuple-element.18), channel_id=2, replica_groups=mesh['z3'=2,'z2'=2,'z1'=2,'z0'=2,'y1'=2,'y0'=2,'x1'=2,'x0'=2,'c'=2] {'y0'}, dimensions={0}, use_global_device_ids=true | all-gather | bytes 122880 | tf_op jit(solution)/shard_map/all_gather | solution.py:162
  22.4 6.6 %all-gather.1 = bf16[4,160,128]{2,1,0:T(8,128)(2,1)S(1)} all-gather(bf16[2,160,128]{2,1,0:T(8,128)(2,1)S(1)} %bitcast.18), channel_id=3, replica_groups=mesh['z3'=2,'z2'=2,'z1'=2,'z0'=2,'y1'=2,'y0'=2,'x1'=2,'x0'=2,'c'=2] {'y1'}, dimensions={0}, use_global_device_ids=true | all-gather | bytes 245760 | tf_op jit(solution)/shard_map/all_gather | solution.py:162
  29.0 8.7 %all-gather.2 = bf16[4,2,160,128]{3,2,1,0:T(8,128)(2,1)S(1)} all-gather(bf16[2,2,160,128]{3,2,1,0:T(8,128)(2,1)S(1)} %bitcast.17), channel_id=4, replica_groups=mesh['z3'=2,'z2'=2,'z1'=2,'z0'=2,'y1'=2,'y0'=2,'x1'=2,'x0'=2,'c'=2] {'z0'}, dimensions={0}, use_global_device_ids=true | all-gather | bytes 491520 | tf_op jit(solution)/shard_map/all_gather | solution.py:162
  37.6 5.1 %all-to-all-done.q_all = bf16[8,168,128]{2,1,0:T(8,128)(2,1)S(1)} async-done(((bf16[8,168,128]{2,1,0:T(8,128)(2,1)}), bf16[8,168,128]{2,1,0:T(8,128)(2,1)S(1)}, u32[]{:S(2)}, u32[]{:S(2)}) %all-to-all-start) | async-done | bytes 344096 | tf_op jit(solution)/shard_map/all_to_all | solution.py:157
  42.7 3.6 %attend.1 = (bf16[8,104,128]{2,1,0:T(8,128)(2,1)}, bf16[8,160,128]{2,1,0:T(8,128)(2,1)S(1)}) custom-call(bf16[8,168,128]{2,1,0:T(8,128)(2,1)S(1)} %all-to-all-done.q_all, bf16[8,160,128]{2,1,0:T(8,128)(2,1)S(1)} %bitcast.15), custom_call_target="tpu_custom_call" | custom-call | tf_op jit(solution)/shard_map/attend/pallas_call | solution.py:147
  46.3 13.0 %all_to_all.20.dkv = bf16[8,160,128]{2,1,0:T(8,128)(2,1)S(1)} all-to-all(bf16[8,160,128]{2,1,0:T(8,128)(2,1)S(1)} %get-tuple-element.19), channel_id=1, replica_groups=mesh['z3'=2,'z2'=2,'z1'=2,'z0'=2,'y1'=2,'y0'=2,'x1'=2,'x0'=2,'c'=2] {'z0..., dimensions={0} | all-to-all | bytes 655360 | tf_op jit(solution)/shard_map/all_to_all | solution.py:157
  59.3 0.7 finish_keys.1
  59.9 9.0 %all_to_all.21.weight = bf16[8,64,128]{2,1,0:T(8,128)(2,1)S(1)} all-to-all(bf16[8,64,128]{2,1,0:T(8,128)(2,1)S(1)} %get-tuple-element.21), channel_id=1, replica_groups=mesh['z3'=2,'z2'=2,'z1'=2,'z0'=2,'y1'=2,'y0'=2,'x1'=2,'x0'=2,'c'=2] {'z0..., dimensions={0} | all-to-all | bytes 262144 | tf_op jit(solution)/shard_map/all_to_all | solution.py:157
  68.9 0.6 join_far.1
  69.5 6.1 %all-to-all-start.3 = ((bf16[8,104,128]{2,1,0:T(8,128)(2,1)}), bf16[8,104,128]{2,1,0:T(8,128)(2,1)S(1)}, u32[]{:S(2)}, u32[]{:S(2)}) async-start(bf16[8,104,128]{2,1,0:T(8,128)(2,1)} %join_far.1), calls=%async_computation.3 | async-start | bytes 425984 | tf_op jit(solution)/shard_map/all_to_all | solution.py:157
  75.6 1.8 %all-gather.3 = f32[64,128]{1,0:T(8,128)S(1)} all-gather(f32[32,128]{1,0:T(8,128)S(1)} %get-tuple-element.23), channel_id=5, replica_groups=mesh['z3'=2,'z2'=2,'z1'=2,'z0'=2,'y1'=2,'y0'=2,'x1'=2,'x0'=2,'c'=2] {'c'}, dimensions={0}, use_global_device_ids=true | all-gather | bytes 49152 | tf_op jit(solution)/shard_map/all_gather | solution.py:162
  77.4 4.6 %all-gather.4 = f32[4,32,128]{2,1,0:T(8,128)S(1)} all-gather(f32[2,32,128]{2,1,0:T(8,128)S(1)} %bitcast.20), channel_id=6, replica_groups=mesh['z3'=2,'z2'=2,'z1'=2,'z0'=2,'y1'=2,'y0'=2,'x1'=2,'x0'=2,'c'=2] {'x0'}, dimensions={0}, use_global_device_ids=true | all-gather | bytes 98304 | tf_op jit(solution)/shard_map/all_gather | solution.py:162
  82.0 6.4 %all-gather.5 = f32[4,2,32,128]{3,2,1,0:T(8,128)S(1)} all-gather(f32[2,2,32,128]{3,2,1,0:T(8,128)S(1)} %bitcast.19), channel_id=7, replica_groups=mesh['z3'=2,'z2'=2,'z1'=2,'z0'=2,'y1'=2,'y0'=2,'x1'=2,'x0'=2,'c'=2] {'x1'}, dimensions={0}, use_global_device_ids=true | all-gather | bytes 196608 | tf_op jit(solution)/shard_map/all_gather | solution.py:162
  88.4 4.3 %all-to-all-done.3.far = bf16[8,104,128]{2,1,0:T(8,128)(2,1)S(1)} async-done(((bf16[8,104,128]{2,1,0:T(8,128)(2,1)}), bf16[8,104,128]{2,1,0:T(8,128)(2,1)S(1)}, u32[]{:S(2)}, u32[]{:S(2)}) %all-to-all-start.3) | async-done | bytes 213024 | tf_op jit(solution)/shard_map/all_to_all | solution.py:157
  92.7 0.6 finish_rest.1
Async XLA Ops:
  2.6 40.1 %all-to-all-start = ((bf16[8,168,128]{2,1,0:T(8,128)(2,1)}), bf16[8,168,128]{2,1,0:T(8,128)(2,1)S(1)}, u32[]{:S(2)}, u32[]{:S(2)}) async-start(bf16[8,168,128]{2,1,0:T(8,128)(2,1)} %get-tuple-element.17), calls=%async_computation | async-start | bytes 688128 | tf_op jit(solution)/shard_map/all_to_all | solution.py:157
  69.5 23.2 %all-to-all-start.3 = ((bf16[8,104,128]{2,1,0:T(8,128)(2,1)}), bf16[8,104,128]{2,1,0:T(8,128)(2,1)S(1)}, u32[]{:S(2)}, u32[]{:S(2)}) async-start(bf16[8,104,128]{2,1,0:T(8,128)(2,1)} %join_far.1), calls=%async_computation.3 | async-start | bytes 425984 | tf_op jit(solution)/shard_map/all_to_all | solution.py:157

commit v6 on v4

--- a/solution.py
+++ b/solution.py
@@ -12,17 +12,22 @@
 VALUE_DIM = 64
 HEAD_DIM = NOPE_DIM + ROPE_DIM
 SCALE = HEAD_DIM**-0.5
-PAD = 16
+PAD = 8
+FAR_ROWS = HEAD_DIM + 8
 Q_ROWS = HEAD_DIM + PAD + VALUE_DIM
 K_ROWS = HEAD_DIM + VALUE_DIM
 BF = jnp.bfloat16
 F32 = jnp.float32
 
-FAR = ("z3", "z2", "z1")
-NEAR = ("z0", "y1", "y0")
+FAR = ("z1", "z2", "z3")
+NEAR = ("y0", "y1", "z0")
 HEADS_AXIS = ("x1", "x0", "c")
 GROUP = 8
 TOK = 128
+
+
+def reverse(index):
+    return (index & 1) * 4 + (index & 2) + index // 4
 
 
 def three_parts(row):
@@ -33,7 +38,8 @@
     return high.astype(F32), middle.astype(F32), low.astype(F32)
 
 
-def prepare(latents, rot_key, weight, queries, logs, outputs, grads, k_out, q_out):
+def prepare(latents, rot_key, weight, queries, logs, outputs, grads, k_out, q_out, latents_out):
+    latents_out[...] = latents[...]
     joined = lax.dot_general(
         latents[...], weight[...], (((1,), (0,)), ((), ())), preferred_element_type=F32
     )
@@ -66,7 +72,7 @@
         tok = q_block.astype(F32).T
         q_tok[at, :] = tok[:, :HEAD_DIM].astype(BF)
         g_tok[at, :] = tok[:, HEAD_DIM + PAD :].astype(BF)
-        k_block = k_all[(i % 4) * 2 + i // 4]
+        k_block = k_all[reverse(i)]
         k_t[:, at] = k_block[:HEAD_DIM]
         ktok = k_block.astype(F32).T
         k_tok[at, :] = jnp.concatenate([ktok[:, :HEAD_DIM], key_pad], axis=1).astype(BF)
@@ -107,7 +113,8 @@
     )
     by_owner = weight.reshape(GROUP, GROUP, 8, TOK)
     for i in range(GROUP):
-        weight_out[i] = by_owner[:, i].reshape(GROUP * 8, TOK).astype(BF)
+        rows = [by_owner[reverse(k), reverse(i)] for k in range(GROUP)]
+        weight_out[i] = jnp.concatenate(rows, axis=0).astype(BF)
 
 
 def join_far(weight, dq, far_out):
@@ -115,10 +122,8 @@
     for i in range(1, GROUP):
         total = total + weight[i].astype(F32)
     for i in range(GROUP):
-        rows = total[i * 8 : (i + 1) * 8]
-        high = rows.astype(BF).astype(F32)
         far_out[i, :HEAD_DIM] = dq[i]
-        far_out[i, HEAD_DIM:] = jnp.concatenate([high, rows - high], axis=0).astype(BF)
+        far_out[i, HEAD_DIM:] = total[i * 8 : (i + 1) * 8].astype(BF)
 
 
 def finish_rest(far, rot, query_grad, weight_grad, rot_grad):
@@ -128,7 +133,7 @@
         total = total + far[i].astype(F32)
         around = around + rot[i]
     query_grad[...] = total[:HEAD_DIM].astype(BF)
-    weight_grad[...] = total[HEAD_DIM : HEAD_DIM + 8] + total[HEAD_DIM + 8 :]
+    weight_grad[...] = total[HEAD_DIM:]
     rot_grad[...] = around
 
 
@@ -156,16 +161,14 @@
 
 def per_device(queries, latents, rot_key, kv_weight, log_sums, outputs, out_grad):
     total = GROUP * TOK
-    k_send, q_send = call(
+    k_send, q_send, latents_kept = call(
         prepare,
         (latents, rot_key.T, kv_weight, queries.T, log_sums.T, outputs.T, out_grad.T),
-        [((K_ROWS, TOK), BF, True), ((GROUP, Q_ROWS, TOK), BF, False)],
+        [((K_ROWS, TOK), BF, True), ((GROUP, Q_ROWS, TOK), BF, False), (latents.shape, BF, True)],
         "prepare",
     )
-    k_pair = gather_pairs(k_send, ("z0",))
-    q_send, k_pair = lax.optimization_barrier((q_send, k_pair))
     q_all = exchange(q_send, FAR)
-    k_all = close(gather_pairs(k_pair, ("y0", "y1")).reshape(GROUP, K_ROWS, TOK))
+    k_all = close(gather_pairs(k_send, NEAR).reshape(GROUP, K_ROWS, TOK))
     dq, dkv = call(
         attend,
         (q_all, k_all),
@@ -187,7 +190,7 @@
     )
     key_grad, value_grad, rot_send, weight_send = call(
         finish_keys,
-        (exchange(dkv, NEAR), latents),
+        (exchange(dkv, NEAR), close(latents_kept)),
         [
             ((NOPE_DIM, TOK), BF, False),
             ((VALUE_DIM, TOK), BF, False),
@@ -200,7 +203,7 @@
     (far_send,) = call(
         join_far,
         (exchange(weight_send, NEAR), close(dq)),
-        [((GROUP, HEAD_DIM + 16, TOK), BF, True)],
+        [((GROUP, FAR_ROWS, TOK), BF, False)],
         "join_far",
     )
     query_grad, weight_grad, rot_grad = call(
@@ -213,7 +216,7 @@
 
 
 def solution(mesh):
-    sp, tp = FAR + NEAR, HEADS_AXIS
+    sp, tp = FAR[::-1] + NEAR[::-1], HEADS_AXIS
     split = Mesh(mesh.devices.reshape((2,) * 9), sp + tp)
     placed = (P(sp, tp), P(sp, None), P(sp, None), P(None, tp), P(sp, tp), P(sp, tp), P(sp, tp))
     return jax.shard_map(

time: 95.5 us -> 90.3 us (0.946)
  waiting for transfers between devices: 15.4 us -> 1.04 us
  starting transfers between devices: 19.3 us -> 25.9 us
  blocking collectives: 51.9 us -> 55.3 us
    all_to_all x2, waiting for transfers between devices: 15.4 us -> 1.04 us  [exchange(): lax.all_to_all(x, axes, split_axis=0, concat_axis=0, tiled=True)]
    all_to_all x2, starting transfers between devices: 19.3 us -> 25.9 us  [exchange(): lax.all_to_all(x, axes, split_axis=0, concat_axis=0, tiled=True)]
    all_gather x6, blocking collectives: 30 us -> 33.3 us  [gather_pairs(): x = lax.all_gather(x, axis, axis=0)]
  transfers between devices with their start and end apart: 2 -> 2, of which waited for: 2 -> 1; matrix products, arithmetic and copies ran while one was open for 0% -> 0% of each run, Pallas kernels for 0% -> 0%
where the time goes in v6:
time: 90.3 us; the launch traced here: 89.8 us
  blocking collectives  55.3 us (61%)
  starting transfers between devices  25.9 us (29%)
  Pallas kernels  6.86 us (8%)
  waiting for transfers between devices  1.04 us (1%)
    all_gather x6, blocking collectives, gather_pairs(): x = lax.all_gather(x, axis, axis=0)  33.3 us
    all_to_all x2, starting transfers between devices, exchange(): lax.all_to_all(x, axes, split_axis=0, concat_axis=0, tiled=True)  25.9 us
    all_to_all x2, blocking collectives, exchange(): lax.all_to_all(x, axes, split_axis=0, concat_axis=0, tiled=True)  22.1 us
    pallas_call x5, Pallas kernels, call(): pl.pallas_call(body, out_shape=shapes, scratch_shapes=list(scratch), name...  6.86 us
  transfers between devices with their start and end apart: 2, of which 1 were waited for; matrix products, arithmetic and copies ran while one was open for 0% of the time, Pallas kernels for 0%

profile of v6, /device:TPU:6, one launch (start us, length us, event | category | flops | bytes accessed | tf_op | source)
XLA Modules:
  0.0 89.8 jit_solution(18389613438971765126)
XLA Ops:
  0.6 2.0 %prepare.1 = (bf16[160,128]{1,0:T(8,128)(2,1)S(1)}, bf16[8,168,128]{2,1,0:T(8,128)(2,1)}, bf16[128,512]{1,0:T(8,128)(2,1)S(1)}) custom-call(bf16[128,512]{1,0:T(8,128)(2,1)} %latents.1, bf16[32,128]{1,0:T(8,128)(2,1)} %bitcast.24, bf16[512,128]{1,0:T(8,128)(2,1)} %weight.1, bf16[96,128]{1,0:T(8,128)(2,1)} %bitcast.21, f32[1,128]{1,0:T(1,128)} %bitcast.25, ...), custom_call_target="tpu_custom_call" | custom-call | tf_op jit(solution)/shard_map/prepare/pallas_call | solution.py:145
  2.6 15.1 %all-to-all-start = ((bf16[8,168,128]{2,1,0:T(8,128)(2,1)}), bf16[8,168,128]{2,1,0:T(8,128)(2,1)S(1)}, u32[]{:S(2)}, u32[]{:S(2)}) async-start(bf16[8,168,128]{2,1,0:T(8,128)(2,1)} %get-tuple-element.17), calls=%async_computation | async-start | bytes 688128 | tf_op jit(solution)/shard_map/all_to_all | solution.py:153
  17.7 4.7 %all-gather = bf16[320,128]{1,0:T(8,128)(2,1)S(1)} all-gather(bf16[160,128]{1,0:T(8,128)(2,1)S(1)} %get-tuple-element.18), channel_id=2, replica_groups=mesh['z3'=2,'z2'=2,'z1'=2,'z0'=2,'y1'=2,'y0'=2,'x1'=2,'x0'=2,'c'=2] {'y0'}, dimensions={0}, use_global_device_ids=true | all-gather | bytes 122880 | tf_op jit(solution)/shard_map/all_gather | solution.py:158
  22.4 6.6 %all-gather.1 = bf16[4,160,128]{2,1,0:T(8,128)(2,1)S(1)} all-gather(bf16[2,160,128]{2,1,0:T(8,128)(2,1)S(1)} %bitcast.18), channel_id=3, replica_groups=mesh['z3'=2,'z2'=2,'z1'=2,'z0'=2,'y1'=2,'y0'=2,'x1'=2,'x0'=2,'c'=2] {'y1'}, dimensions={0}, use_global_device_ids=true | all-gather | bytes 245760 | tf_op jit(solution)/shard_map/all_gather | solution.py:158
  29.0 9.2 %all-gather.2 = bf16[4,2,160,128]{3,2,1,0:T(8,128)(2,1)S(1)} all-gather(bf16[2,2,160,128]{3,2,1,0:T(8,128)(2,1)S(1)} %bitcast.17), channel_id=4, replica_groups=mesh['z3'=2,'z2'=2,'z1'=2,'z0'=2,'y1'=2,'y0'=2,'x1'=2,'x0'=2,'c'=2] {'z0'}, dimensions={0}, use_global_device_ids=true | all-gather | bytes 491520 | tf_op jit(solution)/shard_map/all_gather | solution.py:158
  38.2 0.0 all-to-all-done.q_all
  38.2 2.9 %attend.1 = (bf16[8,96,128]{2,1,0:T(8,128)(2,1)S(1)}, bf16[8,160,128]{2,1,0:T(8,128)(2,1)S(1)}) custom-call(bf16[8,168,128]{2,1,0:T(8,128)(2,1)S(1)} %all-to-all-done.q_all, bf16[8,160,128]{2,1,0:T(8,128)(2,1)S(1)} %bitcast.15), custom_call_target="tpu_custom_call" | custom-call | tf_op jit(solution)/shard_map/attend/pallas_call | solution.py:145
  41.1 12.9 %all_to_all.20.dkv = bf16[8,160,128]{2,1,0:T(8,128)(2,1)S(1)} all-to-all(bf16[8,160,128]{2,1,0:T(8,128)(2,1)S(1)} %get-tuple-element.19), channel_id=1, replica_groups=mesh['z3'=2,'z2'=2,'z1'=2,'z0'=2,'y1'=2,'y0'=2,'x1'=2,'x0'=2,'c'=2] {'y0..., dimensions={0} | all-to-all | bytes 655360 | tf_op jit(solution)/shard_map/all_to_all | solution.py:153
  54.0 0.7 finish_keys.1
  54.7 9.1 %all_to_all.21.weight = bf16[8,64,128]{2,1,0:T(8,128)(2,1)S(1)} all-to-all(bf16[8,64,128]{2,1,0:T(8,128)(2,1)S(1)} %get-tuple-element.21), channel_id=1, replica_groups=mesh['z3'=2,'z2'=2,'z1'=2,'z0'=2,'y1'=2,'y0'=2,'x1'=2,'x0'=2,'c'=2] {'y0..., dimensions={0} | all-to-all | bytes 262144 | tf_op jit(solution)/shard_map/all_to_all | solution.py:153
  63.8 0.7 join_far.1
  64.5 10.8 %all-to-all-start.3 = ((bf16[8,104,128]{2,1,0:T(8,128)(2,1)}), bf16[8,104,128]{2,1,0:T(8,128)(2,1)S(1)}, u32[]{:S(2)}, u32[]{:S(2)}) async-start(bf16[8,104,128]{2,1,0:T(8,128)(2,1)} %join_far.1), calls=%async_computation.3 | async-start | bytes 425984 | tf_op jit(solution)/shard_map/all_to_all | solution.py:153
  75.3 1.8 %all-gather.3 = f32[64,128]{1,0:T(8,128)S(1)} all-gather(f32[32,128]{1,0:T(8,128)S(1)} %get-tuple-element.23), channel_id=5, replica_groups=mesh['z3'=2,'z2'=2,'z1'=2,'z0'=2,'y1'=2,'y0'=2,'x1'=2,'x0'=2,'c'=2] {'c'}, dimensions={0}, use_global_device_ids=true | all-gather | bytes 49152 | tf_op jit(solution)/shard_map/all_gather | solution.py:158
  77.1 4.6 %all-gather.4 = f32[4,32,128]{2,1,0:T(8,128)S(1)} all-gather(f32[2,32,128]{2,1,0:T(8,128)S(1)} %bitcast.20), channel_id=6, replica_groups=mesh['z3'=2,'z2'=2,'z1'=2,'z0'=2,'y1'=2,'y0'=2,'x1'=2,'x0'=2,'c'=2] {'x0'}, dimensions={0}, use_global_device_ids=true | all-gather | bytes 98304 | tf_op jit(solution)/shard_map/all_gather | solution.py:158
  81.7 6.4 %all-gather.5 = f32[4,2,32,128]{3,2,1,0:T(8,128)S(1)} all-gather(f32[2,2,32,128]{3,2,1,0:T(8,128)S(1)} %bitcast.19), channel_id=7, replica_groups=mesh['z3'=2,'z2'=2,'z1'=2,'z0'=2,'y1'=2,'y0'=2,'x1'=2,'x0'=2,'c'=2] {'x1'}, dimensions={0}, use_global_device_ids=true | all-gather | bytes 196608 | tf_op jit(solution)/shard_map/all_gather | solution.py:158
  88.1 1.0 %all-to-all-done.3.far = bf16[8,104,128]{2,1,0:T(8,128)(2,1)S(1)} async-done(((bf16[8,104,128]{2,1,0:T(8,128)(2,1)}), bf16[8,104,128]{2,1,0:T(8,128)(2,1)S(1)}, u32[]{:S(2)}, u32[]{:S(2)}) %all-to-all-start.3) | async-done | bytes 213024 | tf_op jit(solution)/shard_map/all_to_all | solution.py:153
  89.1 0.6 finish_rest.1
Async XLA Ops:
  2.6 35.6 %all-to-all-start = ((bf16[8,168,128]{2,1,0:T(8,128)(2,1)}), bf16[8,168,128]{2,1,0:T(8,128)(2,1)S(1)}, u32[]{:S(2)}, u32[]{:S(2)}) async-start(bf16[8,168,128]{2,1,0:T(8,128)(2,1)} %get-tuple-element.17), calls=%async_computation | async-start | bytes 688128 | tf_op jit(solution)/shard_map/all_to_all | solution.py:153
  64.5 24.7 %all-to-all-start.3 = ((bf16[8,104,128]{2,1,0:T(8,128)(2,1)}), bf16[8,104,128]{2,1,0:T(8,128)(2,1)S(1)}, u32[]{:S(2)}, u32[]{:S(2)}) async-start(bf16[8,104,128]{2,1,0:T(8,128)(2,1)} %join_far.1), calls=%async_computation.3 | async-start | bytes 425984 | tf_op jit(solution)/shard_map/all_to_all | solution.py:153

commit v7 on v6

--- a/solution.py
+++ b/solution.py
@@ -6,6 +6,7 @@
 from jax.experimental import pallas as pl
 from jax.experimental.pallas import tpu as pltpu
 from jax.sharding import Mesh, PartitionSpec as P
+
 
 NOPE_DIM = 64
 ROPE_DIM = 32
@@ -60,7 +61,12 @@
         q_out[i] = block
 
 
-def attend(q_all, k_all, dq_out, dkv_out, q_t, q_tok, g_tok, k_t, k_tok, v_tok, dq_acc, dk_acc, dv_acc, dscores, probs_b):
+def pair(own, other, out):
+    out[0] = own[...]
+    out[1] = other[...]
+
+
+def attend(side, q_all, k_all, dq_out, dkv_out, q_t, q_tok, g_tok, k_t, k_tok, v_tok, dq_acc, dk_acc, dv_acc, dscores, probs_b):
     total = GROUP * TOK
     lane = lax.broadcasted_iota(jnp.int32, (TOK, PAD), 1)
     key_pad = jnp.where(lane < 3, 1.0, 0.0).astype(F32)
@@ -72,7 +78,8 @@
         tok = q_block.astype(F32).T
         q_tok[at, :] = tok[:, :HEAD_DIM].astype(BF)
         g_tok[at, :] = tok[:, HEAD_DIM + PAD :].astype(BF)
-        k_block = k_all[reverse(i)]
+        y_index = (i & 2) + i // 4
+        k_block = k_all[y_index * 2 + (side[0] ^ (i & 1))]
         k_t[:, at] = k_block[:HEAD_DIM]
         ktok = k_block.astype(F32).T
         k_tok[at, :] = jnp.concatenate([ktok[:, :HEAD_DIM], key_pad], axis=1).astype(BF)
@@ -137,12 +144,12 @@
     rot_grad[...] = around
 
 
-def call(body, args, outs, name, scratch=()):
+def call(body, args, outs, scratch=(), **more):
     shapes = [
         pltpu.VMEM(shape, kind) if near else jax.ShapeDtypeStruct(shape, kind)
         for shape, kind, near in outs
     ]
-    return pl.pallas_call(body, out_shape=shapes, scratch_shapes=list(scratch), name=name)(*args)
+    return pl.pallas_call(body, out_shape=shapes, scratch_shapes=list(scratch), **more)(*args)
 
 
 def close(x):
@@ -165,15 +172,16 @@
         prepare,
         (latents, rot_key.T, kv_weight, queries.T, log_sums.T, outputs.T, out_grad.T),
         [((K_ROWS, TOK), BF, True), ((GROUP, Q_ROWS, TOK), BF, False), (latents.shape, BF, True)],
-        "prepare",
-    )
+    )
+    k_other = lax.ppermute(k_send, "z0", ((0, 1), (1, 0)))
     q_all = exchange(q_send, FAR)
-    k_all = close(gather_pairs(k_send, NEAR).reshape(GROUP, K_ROWS, TOK))
+    (k_pair,) = call(pair, (close(k_send), close(k_other)), [((2, K_ROWS, TOK), BF, True)])
+    k_all = close(gather_pairs(k_pair, NEAR[:2]).reshape(GROUP, K_ROWS, TOK))
+    side = lax.axis_index("z0").astype(jnp.int32).reshape(1)
     dq, dkv = call(
         attend,
-        (q_all, k_all),
+        (side, q_all, k_all),
         [((GROUP, HEAD_DIM, TOK), BF, True), ((GROUP, K_ROWS, TOK), BF, True)],
-        "attend",
         [
             pltpu.VMEM((Q_ROWS, total), BF),
             pltpu.VMEM((total, HEAD_DIM), BF),
@@ -187,6 +195,7 @@
             pltpu.VMEM((total, total), BF),
             pltpu.VMEM((total, total), BF),
         ],
+        in_specs=[pl.BlockSpec(memory_space=where) for where in (pltpu.SMEM, pltpu.VMEM, pltpu.VMEM)],
     )
     key_grad, value_grad, rot_send, weight_send = call(
         finish_keys,
@@ -197,20 +206,15 @@
             ((ROPE_DIM, TOK), F32, True),
             ((GROUP, GROUP * 8, TOK), BF, True),
         ],
-        "finish_keys",
     )
     rot_all = close(gather_pairs(rot_send, HEADS_AXIS[::-1]).reshape(GROUP, ROPE_DIM, TOK))
     (far_send,) = call(
-        join_far,
-        (exchange(weight_send, NEAR), close(dq)),
-        [((GROUP, FAR_ROWS, TOK), BF, False)],
-        "join_far",
+        join_far, (exchange(weight_send, NEAR), close(dq)), [((GROUP, FAR_ROWS, TOK), BF, False)]
     )
     query_grad, weight_grad, rot_grad = call(
         finish_rest,
         (exchange(far_send, FAR), rot_all),
         [((HEAD_DIM, TOK), BF, False), ((8, TOK), F32, False), ((ROPE_DIM, TOK), F32, False)],
-        "finish_rest",
     )
     return query_grad.T, key_grad.T, value_grad.T, rot_grad.T, weight_grad
 

time: 90.3 us -> 98.8 us (1.094)
  waiting for transfers between devices: 1.04 us -> 11.5 us
  blocking collectives: 55.3 us -> 47.3 us
  starting transfers between devices: 25.9 us -> 31.9 us
    ppermute x0 -> x1, waiting for transfers between devices: none -> 11.4 us  [per_device(): k_other = lax.ppermute(k_send, 'z0', ((0, 1), (1, 0)))]
    all_gather x6 -> x5, blocking collectives: 33.3 us -> 25.5 us  [gather_pairs(): x = lax.all_gather(x, axis, axis=0)]
    all_to_all x2, starting transfers between devices: 25.9 us -> 29 us  [exchange(): lax.all_to_all(x, axes, split_axis=0, concat_axis=0, tiled=True)]
    ppermute x0 -> x1, starting transfers between devices: none -> 2.91 us  [per_device(): k_other = lax.ppermute(k_send, 'z0', ((0, 1), (1, 0)))]
    pallas_call x5 -> x6, Pallas kernels: 6.86 us -> 6.89 us  [call(): pl.pallas_call(body, out_shape=shapes, scratch_shapes=list(scratch), **more)]
  transfers between devices with their start and end apart: 2 -> 3, of which waited for: 1 -> 2; matrix products, arithmetic and copies ran while one was open for 0% -> 0% of each run, Pallas kernels for 0% -> 0%
where the time goes in v7:
time: 98.8 us; the launch traced here: 98.3 us
  blocking collectives  47.3 us (48%)
  starting transfers between devices  31.9 us (32%)
  waiting for transfers between devices  11.5 us (12%)
  Pallas kernels  6.89 us (7%)
    all_to_all x2, starting transfers between devices, exchange(): lax.all_to_all(x, axes, split_axis=0, concat_axis=0, tiled=True)  29 us
    all_gather x5, blocking collectives, gather_pairs(): x = lax.all_gather(x, axis, axis=0)  25.5 us
    all_to_all x2, blocking collectives, exchange(): lax.all_to_all(x, axes, split_axis=0, concat_axis=0, tiled=True)  21.9 us
    ppermute x1, waiting for transfers between devices, per_device(): k_other = lax.ppermute(k_send, 'z0', ((0, 1), (1, 0)))  11.4 us
    pallas_call x6, Pallas kernels, call(): pl.pallas_call(body, out_shape=shapes, scratch_shapes=list(scratch), **more)  6.89 us
    ppermute x1, starting transfers between devices, per_device(): k_other = lax.ppermute(k_send, 'z0', ((0, 1), (1, 0)))  2.91 us
  transfers between devices with their start and end apart: 3, of which 2 were waited for; matrix products, arithmetic and copies ran while one was open for 0% of the time, Pallas kernels for 0%

profile of v7, /device:TPU:6, one launch (start us, length us, event | category | flops | bytes accessed | tf_op | source)
XLA Modules:
  0.0 98.3 jit_solution(13038479808396947511)
XLA Ops:
  0.6 2.0 %shard_map.110 = (bf16[160,128]{1,0:T(8,128)(2,1)S(1)}, bf16[8,168,128]{2,1,0:T(8,128)(2,1)}, bf16[128,512]{1,0:T(8,128)(2,1)S(1)}) custom-call(bf16[128,512]{1,0:T(8,128)(2,1)} %latents.1, bf16[32,128]{1,0:T(8,128)(2,1)} %bitcast.23, bf16[512,128]{1,0:T(8,128)(2,1)} %weight.1, bf16[96,128]{1,0:T(8,128)(2,1)} %bitcast.20, f32[1,128]{1,0:T(1,128)} %bitcast.24, ...), custom_call_target="tpu_custom_call" | custom-call | tf_op jit(solution)/shard_map/pallas_call | solution.py:152
  2.6 15.1 %all-to-all-start = ((bf16[8,168,128]{2,1,0:T(8,128)(2,1)}), bf16[8,168,128]{2,1,0:T(8,128)(2,1)S(1)}, u32[]{:S(2)}, u32[]{:S(2)}) async-start(bf16[8,168,128]{2,1,0:T(8,128)(2,1)} %get-tuple-element.17), calls=%async_computation | async-start | bytes 688128 | tf_op jit(solution)/shard_map/all_to_all | solution.py:160
  17.7 2.9 %collective-permute-start = (bf16[160,128]{1,0:T(8,128)(2,1)S(1)}, bf16[160,128]{1,0:T(8,128)(2,1)S(1)}, u32[]{:S(2)}, u32[]{:S(2)}) collective-permute-start(bf16[160,128]{1,0:T(8,128)(2,1)S(1)} %get-tuple-element.18.own), channel_id=1, source_target_pairs={{0,32},{32,0},{1,33},{33,1},{2,34},{34,2},{3,35},{35,3},{4,36},{36... | collective-permute-start | bytes 122888 | tf_op jit(solution)/shard_map/ppermute | solution.py:176
  20.6 11.4 %collective-permute-done.other = bf16[160,128]{1,0:T(8,128)(2,1)S(1)} collective-permute-done((bf16[160,128]{1,0:T(8,128)(2,1)S(1)}, bf16[160,128]{1,0:T(8,128)(2,1)S(1)}, u32[]{:S(2)}, u32[]{:S(2)}) %collective-permute-start) | collective-permute-done | bytes 40992 | tf_op jit(solution)/shard_map/ppermute | solution.py:176
  32.0 5.1 %all-gather = bf16[4,160,128]{2,1,0:T(8,128)(2,1)S(1)} all-gather(bf16[2,160,128]{2,1,0:T(8,128)(2,1)S(1)} %shard_map.111), channel_id=2, replica_groups=mesh['z3'=2,'z2'=2,'z1'=2,'z0'=2,'y1'=2,'y0'=2,'x1'=2,'x0'=2,'c'=2] {'y0'}, dimensions={0}, use_global_device_ids=true | all-gather | bytes 245760 | tf_op jit(solution)/shard_map/all_gather | solution.py:165
  37.1 7.6 %all-gather.1 = bf16[4,2,160,128]{3,2,1,0:T(8,128)(2,1)S(1)} all-gather(bf16[2,2,160,128]{3,2,1,0:T(8,128)(2,1)S(1)} %bitcast.17), channel_id=3, replica_groups=mesh['z3'=2,'z2'=2,'z1'=2,'z0'=2,'y1'=2,'y0'=2,'x1'=2,'x0'=2,'c'=2] {'y1'}, dimensions={0}, use_global_device_ids=true | all-gather | bytes 491520 | tf_op jit(solution)/shard_map/all_gather | solution.py:165
  44.7 0.0 all-to-all-done.q_all
  44.7 2.9 %shard_map.112 = (bf16[8,96,128]{2,1,0:T(8,128)(2,1)S(1)}, bf16[8,160,128]{2,1,0:T(8,128)(2,1)S(1)}) custom-call(s32[1]{0:T(128)} %bitcast.side, bf16[8,168,128]{2,1,0:T(8,128)(2,1)S(1)} %all-to-all-done.q_all, bf16[8,160,128]{2,1,0:T(8,128)(2,1)S(1)} %bitcast.15), custom_call_target="tpu_custom_call" | custom-call | tf_op jit(solution)/shard_map/pallas_call | solution.py:152
  47.6 12.7 %all_to_all.20.dkv = bf16[8,160,128]{2,1,0:T(8,128)(2,1)S(1)} all-to-all(bf16[8,160,128]{2,1,0:T(8,128)(2,1)S(1)} %get-tuple-element.19), channel_id=1, replica_groups=mesh['z3'=2,'z2'=2,'z1'=2,'z0'=2,'y1'=2,'y0'=2,'x1'=2,'x0'=2,'c'=2] {'y0..., dimensions={0} | all-to-all | bytes 655360 | tf_op jit(solution)/shard_map/all_to_all | solution.py:160
  60.4 0.7 shard_map.113
  61.0 9.1 %all_to_all.21.weight = bf16[8,64,128]{2,1,0:T(8,128)(2,1)S(1)} all-to-all(bf16[8,64,128]{2,1,0:T(8,128)(2,1)S(1)} %get-tuple-element.21), channel_id=1, replica_groups=mesh['z3'=2,'z2'=2,'z1'=2,'z0'=2,'y1'=2,'y0'=2,'x1'=2,'x0'=2,'c'=2] {'y0..., dimensions={0} | all-to-all | bytes 262144 | tf_op jit(solution)/shard_map/all_to_all | solution.py:160
  70.1 0.7 shard_map.114
  70.9 13.9 %all-to-all-start.3 = ((bf16[8,104,128]{2,1,0:T(8,128)(2,1)}), bf16[8,104,128]{2,1,0:T(8,128)(2,1)S(1)}, u32[]{:S(2)}, u32[]{:S(2)}) async-start(bf16[8,104,128]{2,1,0:T(8,128)(2,1)} %shard_map.114), calls=%async_computation.3 | async-start | bytes 425984 | tf_op jit(solution)/shard_map/all_to_all | solution.py:160
  84.8 1.8 %all-gather.2 = f32[64,128]{1,0:T(8,128)S(1)} all-gather(f32[32,128]{1,0:T(8,128)S(1)} %get-tuple-element.23), channel_id=4, replica_groups=mesh['z3'=2,'z2'=2,'z1'=2,'z0'=2,'y1'=2,'y0'=2,'x1'=2,'x0'=2,'c'=2] {'c'}, dimensions={0}, use_global_device_ids=true | all-gather | bytes 49152 | tf_op jit(solution)/shard_map/all_gather | solution.py:165
  86.6 4.6 %all-gather.3 = f32[4,32,128]{2,1,0:T(8,128)S(1)} all-gather(f32[2,32,128]{2,1,0:T(8,128)S(1)} %bitcast.19), channel_id=5, replica_groups=mesh['z3'=2,'z2'=2,'z1'=2,'z0'=2,'y1'=2,'y0'=2,'x1'=2,'x0'=2,'c'=2] {'x0'}, dimensions={0}, use_global_device_ids=true | all-gather | bytes 98304 | tf_op jit(solution)/shard_map/all_gather | solution.py:165
  91.2 6.4 %all-gather.4 = f32[4,2,32,128]{3,2,1,0:T(8,128)S(1)} all-gather(f32[2,2,32,128]{3,2,1,0:T(8,128)S(1)} %bitcast.18), channel_id=6, replica_groups=mesh['z3'=2,'z2'=2,'z1'=2,'z0'=2,'y1'=2,'y0'=2,'x1'=2,'x0'=2,'c'=2] {'x1'}, dimensions={0}, use_global_device_ids=true | all-gather | bytes 196608 | tf_op jit(solution)/shard_map/all_gather | solution.py:165
  97.6 0.1 all-to-all-done.3.far
  97.7 0.6 shard_map.115
  (1 shorter events, 0.0 us)
Async XLA Ops:
  2.6 42.1 %all-to-all-start = ((bf16[8,168,128]{2,1,0:T(8,128)(2,1)}), bf16[8,168,128]{2,1,0:T(8,128)(2,1)S(1)}, u32[]{:S(2)}, u32[]{:S(2)}) async-start(bf16[8,168,128]{2,1,0:T(8,128)(2,1)} %get-tuple-element.17), calls=%async_computation | async-start | bytes 688128 | tf_op jit(solution)/shard_map/all_to_all | solution.py:160
  17.7 14.3 %collective-permute-start = (bf16[160,128]{1,0:T(8,128)(2,1)S(1)}, bf16[160,128]{1,0:T(8,128)(2,1)S(1)}, u32[]{:S(2)}, u32[]{:S(2)}) collective-permute-start(bf16[160,128]{1,0:T(8,128)(2,1)S(1)} %get-tuple-element.18.own), channel_id=1, source_target_pairs={{0,32},{32,0},{1,33},{33,1},{2,34},{34,2},{3,35},{35,3},{4,36},{36... | collective-permute-start | bytes 122888 | tf_op jit(solution)/shard_map/ppermute | solution.py:176
  70.9 26.8 %all-to-all-start.3 = ((bf16[8,104,128]{2,1,0:T(8,128)(2,1)}), bf16[8,104,128]{2,1,0:T(8,128)(2,1)S(1)}, u32[]{:S(2)}, u32[]{:S(2)}) async-start(bf16[8,104,128]{2,1,0:T(8,128)(2,1)} %shard_map.114), calls=%async_computation.3 | async-start | bytes 425984 | tf_op jit(solution)/shard_map/all_to_all | solution.py:160

commit v8 on v7

--- a/solution.py
+++ b/solution.py
@@ -5,7 +5,7 @@
 from jax import lax
 from jax.experimental import pallas as pl
 from jax.experimental.pallas import tpu as pltpu
-from jax.sharding import Mesh, PartitionSpec as P
+from jax.sharding import PartitionSpec as P
 
 
 NOPE_DIM = 64
@@ -20,15 +20,20 @@
 BF = jnp.bfloat16
 F32 = jnp.float32
 
-FAR = ("z1", "z2", "z3")
-NEAR = ("y0", "y1", "z0")
-HEADS_AXIS = ("x1", "x0", "c")
+OUT_ORDER = (8, 0, 12, 4, 10, 2, 14, 6)
+BACK_ORDER = (0, 8, 4, 12, 2, 10, 6, 14)
+OUT, BACK = (
+    [[(z + low) * 4 + y for z in order] for low in range(2) for y in range(4)]
+    for order in (OUT_ORDER, BACK_ORDER)
+)
+NEAR_ORDER = ((0, 0), (1, 0), (0, 2), (1, 2), (0, 1), (1, 1), (0, 3), (1, 3))
+NEAR = [[(high + z) * 4 + y for z, y in NEAR_ORDER] for high in range(0, 16, 2)]
 GROUP = 8
 TOK = 128
 
 
-def reverse(index):
-    return (index & 1) * 4 + (index & 2) + index // 4
+def pairs(count, bit):
+    return [[i, i + bit] for i in range(count) if not i & bit]
 
 
 def three_parts(row):
@@ -78,8 +83,8 @@
         tok = q_block.astype(F32).T
         q_tok[at, :] = tok[:, :HEAD_DIM].astype(BF)
         g_tok[at, :] = tok[:, HEAD_DIM + PAD :].astype(BF)
-        y_index = (i & 2) + i // 4
-        k_block = k_all[y_index * 2 + (side[0] ^ (i & 1))]
+        low, y = NEAR_ORDER[i]
+        k_block = k_all[y * 2 + (side[0] ^ low)]
         k_t[:, at] = k_block[:HEAD_DIM]
         ktok = k_block.astype(F32).T
         k_tok[at, :] = jnp.concatenate([ktok[:, :HEAD_DIM], key_pad], axis=1).astype(BF)
@@ -101,7 +106,7 @@
         dq_acc[:, qs] = jnp.dot(k_t[...], dscores[:, qs], preferred_element_type=F32)
     for i in range(GROUP):
         at = slice(i * TOK, (i + 1) * TOK)
-        dq_out[i] = (dq_acc[:, at] * SCALE).astype(BF)
+        dq_out[BACK_ORDER.index(OUT_ORDER[i])] = (dq_acc[:, at] * SCALE).astype(BF)
         dkv_out[i] = jnp.concatenate(
             [(dk_acc[at, :] * SCALE).T, dv_acc[at, :].T], axis=0
         ).astype(BF)
@@ -120,7 +125,8 @@
     )
     by_owner = weight.reshape(GROUP, GROUP, 8, TOK)
     for i in range(GROUP):
-        rows = [by_owner[reverse(k), reverse(i)] for k in range(GROUP)]
+        low, y = NEAR_ORDER[i]
+        rows = [by_owner[z // 2, low * 4 + y] for z in BACK_ORDER]
         weight_out[i] = jnp.concatenate(rows, axis=0).astype(BF)
 
 
@@ -156,13 +162,13 @@
     return pltpu.with_memory_space_constraint(x, pltpu.VMEM)
 
 
-def exchange(x, axes):
-    return close(lax.all_to_all(x, axes, split_axis=0, concat_axis=0, tiled=True))
-
-
-def gather_pairs(x, axes):
-    for axis in axes:
-        x = lax.all_gather(x, axis, axis=0)
+def exchange(x, groups):
+    return close(lax.all_to_all(x, "sp", 0, 0, axis_index_groups=groups, tiled=True))
+
+
+def gather_pairs(x, axis, count, bits):
+    for bit in bits:
+        x = lax.all_gather(x, axis, axis_index_groups=pairs(count, bit))
     return x
 
 
@@ -173,11 +179,11 @@
         (latents, rot_key.T, kv_weight, queries.T, log_sums.T, outputs.T, out_grad.T),
         [((K_ROWS, TOK), BF, True), ((GROUP, Q_ROWS, TOK), BF, False), (latents.shape, BF, True)],
     )
-    k_other = lax.ppermute(k_send, "z0", ((0, 1), (1, 0)))
-    q_all = exchange(q_send, FAR)
+    k_other = lax.ppermute(k_send, "sp", [(i, i ^ 4) for i in range(64)])
+    q_all = exchange(q_send, OUT)
     (k_pair,) = call(pair, (close(k_send), close(k_other)), [((2, K_ROWS, TOK), BF, True)])
-    k_all = close(gather_pairs(k_pair, NEAR[:2]).reshape(GROUP, K_ROWS, TOK))
-    side = lax.axis_index("z0").astype(jnp.int32).reshape(1)
+    k_all = close(gather_pairs(k_pair, "sp", 64, (1, 2)).reshape(GROUP, K_ROWS, TOK))
+    side = (lax.axis_index("sp") // 4 % 2).astype(jnp.int32).reshape(1)
     dq, dkv = call(
         attend,
         (side, q_all, k_all),
@@ -207,26 +213,24 @@
             ((GROUP, GROUP * 8, TOK), BF, True),
         ],
     )
-    rot_all = close(gather_pairs(rot_send, HEADS_AXIS[::-1]).reshape(GROUP, ROPE_DIM, TOK))
+    rot_all = close(gather_pairs(rot_send, "tp", 8, (1, 2, 4)).reshape(GROUP, ROPE_DIM, TOK))
     (far_send,) = call(
         join_far, (exchange(weight_send, NEAR), close(dq)), [((GROUP, FAR_ROWS, TOK), BF, False)]
     )
     query_grad, weight_grad, rot_grad = call(
         finish_rest,
-        (exchange(far_send, FAR), rot_all),
+        (exchange(far_send, BACK), rot_all),
         [((HEAD_DIM, TOK), BF, False), ((8, TOK), F32, False), ((ROPE_DIM, TOK), F32, False)],
     )
     return query_grad.T, key_grad.T, value_grad.T, rot_grad.T, weight_grad
 
 
 def solution(mesh):
-    sp, tp = FAR[::-1] + NEAR[::-1], HEADS_AXIS
-    split = Mesh(mesh.devices.reshape((2,) * 9), sp + tp)
-    placed = (P(sp, tp), P(sp, None), P(sp, None), P(None, tp), P(sp, tp), P(sp, tp), P(sp, tp))
+    placed = (P("sp", "tp"), P("sp", None), P("sp", None), P(None, "tp"), P("sp", "tp"), P("sp", "tp"), P("sp", "tp"))
     return jax.shard_map(
         per_device,
-        mesh=split,
+        mesh=mesh,
         in_specs=placed,
-        out_specs=(P(sp, tp), P(sp, tp), P(sp, tp), P(sp, None), P(sp, tp)),
+        out_specs=(P("sp", "tp"), P("sp", "tp"), P("sp", "tp"), P("sp", None), P("sp", "tp")),
         check_vma=False,
     )

time: 98.8 us -> 93.6 us (0.947)
  starting transfers between devices: 31.9 us -> 24.7 us
  waiting for transfers between devices: 11.5 us -> 13.6 us
    all_to_all x2, starting transfers between devices: 29 us -> 21.8 us  [exchange(): lax.all_to_all(x, 'sp', 0, 0, axis_index_groups=groups, tiled=True)]
    ppermute x1, waiting for transfers between devices: 11.4 us -> 13.6 us  [per_device(): k_other = lax.ppermute(k_send, 'sp', [(i, i ^ 4) for i in range(64)])]
  transfers between devices with their start and end apart: 3 -> 3, of which waited for: 2 -> 1; matrix products, arithmetic and copies ran while one was open for 0% -> 0% of each run, Pallas kernels for 0% -> 0%
where the time goes in v8:
time: 93.6 us; the launch traced here: 92.9 us
  blocking collectives  47 us (50%)
  starting transfers between devices  24.7 us (26%)
  waiting for transfers between devices  13.6 us (15%)
  Pallas kernels  6.89 us (7%)
    all_gather x5, blocking collectives, gather_pairs(): x = lax.all_gather(x, axis, axis_index_groups=pairs(count, bit))  25.4 us
    all_to_all x2, starting transfers between devices, exchange(): lax.all_to_all(x, 'sp', 0, 0, axis_index_groups=groups, tiled=True)  21.8 us
    all_to_all x2, blocking collectives, exchange(): lax.all_to_all(x, 'sp', 0, 0, axis_index_groups=groups, tiled=True)  21.6 us
    ppermute x1, waiting for transfers between devices, per_device(): k_other = lax.ppermute(k_send, 'sp', [(i, i ^ 4) for i in range(64)])  13.6 us
    pallas_call x6, Pallas kernels, call(): pl.pallas_call(body, out_shape=shapes, scratch_shapes=list(scratch), **more)  6.89 us
    ppermute x1, starting transfers between devices, per_device(): k_other = lax.ppermute(k_send, 'sp', [(i, i ^ 4) for i in range(64)])  2.91 us
  transfers between devices with their start and end apart: 3, of which 1 were waited for; matrix products, arithmetic and copies ran while one was open for 0% of the time, Pallas kernels for 0%

profile of v8, /device:TPU:6, one launch (start us, length us, event | category | flops | bytes accessed | tf_op | source)
XLA Modules:
  0.0 92.9 jit_solution(17707805322791841848)
XLA Ops:
  0.6 2.0 %shard_map.110 = (bf16[160,128]{1,0:T(8,128)(2,1)S(1)}, bf16[8,168,128]{2,1,0:T(8,128)(2,1)}, bf16[128,512]{1,0:T(8,128)(2,1)S(1)}) custom-call(bf16[128,512]{1,0:T(8,128)(2,1)} %latents.1, bf16[32,128]{1,0:T(8,128)(2,1)} %bitcast.23, bf16[512,128]{1,0:T(8,128)(2,1)} %weight.1, bf16[96,128]{1,0:T(8,128)(2,1)} %bitcast.20, f32[1,128]{1,0:T(1,128)} %bitcast.24, ...), custom_call_target="tpu_custom_call" | custom-call | tf_op jit(solution)/shard_map/pallas_call | solution.py:158
  2.6 18.4 %all-to-all-start = ((bf16[8,168,128]{2,1,0:T(8,128)(2,1)}), bf16[8,168,128]{2,1,0:T(8,128)(2,1)S(1)}, u32[]{:S(2)}, u32[]{:S(2)}) async-start(bf16[8,168,128]{2,1,0:T(8,128)(2,1)} %get-tuple-element.17), calls=%async_computation | async-start | bytes 688128 | tf_op jit(solution)/shard_map/all_to_all | solution.py:166
  21.0 2.9 %collective-permute-start = (bf16[160,128]{1,0:T(8,128)(2,1)S(1)}, bf16[160,128]{1,0:T(8,128)(2,1)S(1)}, u32[]{:S(2)}, u32[]{:S(2)}) collective-permute-start(bf16[160,128]{1,0:T(8,128)(2,1)S(1)} %get-tuple-element.18.own), channel_id=1, source_target_pairs={{0,32},{8,40},{16,48},{24,56},{32,0},{40,8},{48,16},{56,24},{64,96... | collective-permute-start | bytes 122888 | tf_op jit(solution)/shard_map/ppermute | solution.py:182
  23.9 13.6 %collective-permute-done.other = bf16[160,128]{1,0:T(8,128)(2,1)S(1)} collective-permute-done((bf16[160,128]{1,0:T(8,128)(2,1)S(1)}, bf16[160,128]{1,0:T(8,128)(2,1)S(1)}, u32[]{:S(2)}, u32[]{:S(2)}) %collective-permute-start) | collective-permute-done | bytes 40992 | tf_op jit(solution)/shard_map/ppermute | solution.py:182
  37.5 5.1 %all-gather = bf16[4,160,128]{2,1,0:T(8,128)(2,1)S(1)} all-gather(bf16[2,160,128]{2,1,0:T(8,128)(2,1)S(1)} %shard_map.111), channel_id=2, replica_groups={{0,8},{16,24},{32,40},{48,56},{64,72},{80,88},{96,104},{112,120},{128,1..., dimensions={0}, use_global_device_ids=true | all-gather | bytes 245760 | tf_op jit(solution)/shard_map/all_gather | solution.py:171
  42.6 7.5 %all-gather.1 = bf16[4,2,160,128]{3,2,1,0:T(8,128)(2,1)S(1)} all-gather(bf16[2,2,160,128]{3,2,1,0:T(8,128)(2,1)S(1)} %bitcast.17), channel_id=3, replica_groups={{0,16},{8,24},{32,48},{40,56},{64,80},{72,88},{96,112},{104,120},{128,1..., dimensions={0}, use_global_device_ids=true | all-gather | bytes 491520 | tf_op jit(solution)/shard_map/all_gather | solution.py:171
  50.1 0.0 all-to-all-done.q_all
  50.1 2.9 %shard_map.112 = (bf16[8,96,128]{2,1,0:T(8,128)(2,1)S(1)}, bf16[8,160,128]{2,1,0:T(8,128)(2,1)S(1)}) custom-call(s32[1]{0:T(128)} %bitcast.side, bf16[8,168,128]{2,1,0:T(8,128)(2,1)S(1)} %all-to-all-done.q_all, bf16[8,160,128]{2,1,0:T(8,128)(2,1)S(1)} %bitcast.15), custom_call_target="tpu_custom_call" | custom-call | tf_op jit(solution)/shard_map/pallas_call | solution.py:158
  53.0 12.5 %all_to_all.20.dkv = bf16[8,160,128]{2,1,0:T(8,128)(2,1)S(1)} all-to-all(bf16[8,160,128]{2,1,0:T(8,128)(2,1)S(1)} %get-tuple-element.19), channel_id=1, replica_groups={{0,32,16,48,8,40,24,56},{64,96,80,112,72,104,88,120},{128,160,144,176,1..., dimensions={0} | all-to-all | bytes 655360 | tf_op jit(solution)/shard_map/all_to_all | solution.py:166
  65.5 0.7 shard_map.113
  66.2 9.1 %all_to_all.21.weight = bf16[8,64,128]{2,1,0:T(8,128)(2,1)S(1)} all-to-all(bf16[8,64,128]{2,1,0:T(8,128)(2,1)S(1)} %get-tuple-element.21), channel_id=1, replica_groups={{0,32,16,48,8,40,24,56},{64,96,80,112,72,104,88,120},{128,160,144,176,1..., dimensions={0} | all-to-all | bytes 262144 | tf_op jit(solution)/shard_map/all_to_all | solution.py:166
  75.3 0.7 shard_map.114
  76.1 3.4 %all-to-all-start.3 = ((bf16[8,104,128]{2,1,0:T(8,128)(2,1)}), bf16[8,104,128]{2,1,0:T(8,128)(2,1)S(1)}, u32[]{:S(2)}, u32[]{:S(2)}) async-start(bf16[8,104,128]{2,1,0:T(8,128)(2,1)} %shard_map.114), calls=%async_computation.3 | async-start | bytes 425984 | tf_op jit(solution)/shard_map/all_to_all | solution.py:166
  79.5 1.8 %all-gather.2 = f32[64,128]{1,0:T(8,128)S(1)} all-gather(f32[32,128]{1,0:T(8,128)S(1)} %get-tuple-element.23), channel_id=4, replica_groups={{0,1},{2,3},{4,5},{6,7},{8,9},{10,11},{12,13},{14,15},{16,17},{18,19},{..., dimensions={0}, use_global_device_ids=true | all-gather | bytes 49152 | tf_op jit(solution)/shard_map/all_gather | solution.py:171
  81.3 4.6 %all-gather.3 = f32[4,32,128]{2,1,0:T(8,128)S(1)} all-gather(f32[2,32,128]{2,1,0:T(8,128)S(1)} %bitcast.19), channel_id=5, replica_groups={{0,2},{1,3},{4,6},{5,7},{8,10},{9,11},{12,14},{13,15},{16,18},{17,19},{..., dimensions={0}, use_global_device_ids=true | all-gather | bytes 98304 | tf_op jit(solution)/shard_map/all_gather | solution.py:171
  85.9 6.4 %all-gather.4 = f32[4,2,32,128]{3,2,1,0:T(8,128)S(1)} all-gather(f32[2,2,32,128]{3,2,1,0:T(8,128)S(1)} %bitcast.18), channel_id=6, replica_groups={{0,4},{1,5},{2,6},{3,7},{8,12},{9,13},{10,14},{11,15},{16,20},{17,21},{..., dimensions={0}, use_global_device_ids=true | all-gather | bytes 196608 | tf_op jit(solution)/shard_map/all_gather | solution.py:171
  92.3 0.0 all-to-all-done.3.far
  92.3 0.6 shard_map.115
  (1 shorter events, 0.0 us)
Async XLA Ops:
  2.6 47.5 %all-to-all-start = ((bf16[8,168,128]{2,1,0:T(8,128)(2,1)}), bf16[8,168,128]{2,1,0:T(8,128)(2,1)S(1)}, u32[]{:S(2)}, u32[]{:S(2)}) async-start(bf16[8,168,128]{2,1,0:T(8,128)(2,1)} %get-tuple-element.17), calls=%async_computation | async-start | bytes 688128 | tf_op jit(solution)/shard_map/all_to_all | solution.py:166
  21.0 16.6 %collective-permute-start = (bf16[160,128]{1,0:T(8,128)(2,1)S(1)}, bf16[160,128]{1,0:T(8,128)(2,1)S(1)}, u32[]{:S(2)}, u32[]{:S(2)}) collective-permute-start(bf16[160,128]{1,0:T(8,128)(2,1)S(1)} %get-tuple-element.18.own), channel_id=1, source_target_pairs={{0,32},{8,40},{16,48},{24,56},{32,0},{40,8},{48,16},{56,24},{64,96... | collective-permute-start | bytes 122888 | tf_op jit(solution)/shard_map/ppermute | solution.py:182
  76.1 16.2 %all-to-all-start.3 = ((bf16[8,104,128]{2,1,0:T(8,128)(2,1)}), bf16[8,104,128]{2,1,0:T(8,128)(2,1)S(1)}, u32[]{:S(2)}, u32[]{:S(2)}) async-start(bf16[8,104,128]{2,1,0:T(8,128)(2,1)} %shard_map.114), calls=%async_computation.3 | async-start | bytes 425984 | tf_op jit(solution)/shard_map/all_to_all | solution.py:166

commit v9 on v8

--- a/solution.py
+++ b/solution.py
@@ -44,7 +44,7 @@
     return high.astype(F32), middle.astype(F32), low.astype(F32)
 
 
-def prepare(latents, rot_key, weight, queries, logs, outputs, grads, k_out, q_out, latents_out):
+def prepare_keys(latents, rot_key, weight, k_out, latents_out):
     latents_out[...] = latents[...]
     joined = lax.dot_general(
         latents[...], weight[...], (((1,), (0,)), ((), ())), preferred_element_type=F32
@@ -53,6 +53,9 @@
     k_out[:NOPE_DIM] = joined_t[:NOPE_DIM]
     k_out[NOPE_DIM:HEAD_DIM] = rot_key[...]
     k_out[HEAD_DIM:] = joined_t[NOPE_DIM:]
+
+
+def prepare_queries(queries, logs, outputs, grads, q_out):
     q_t = queries[...].astype(F32)
     g_t = grads[...].astype(F32)
     delta = jnp.sum(outputs[...].astype(F32) * g_t, axis=0, keepdims=True)
@@ -66,12 +69,7 @@
         q_out[i] = block
 
 
-def pair(own, other, out):
-    out[0] = own[...]
-    out[1] = other[...]
-
-
-def attend(side, q_all, k_all, dq_out, dkv_out, q_t, q_tok, g_tok, k_t, k_tok, v_tok, dq_acc, dk_acc, dv_acc, dscores, probs_b):
+def attend(q_all, k_all, dq_out, dkv_out, q_t, q_tok, g_tok, k_t, k_tok, v_tok, dq_acc, dk_acc, dv_acc, dscores, probs_b):
     total = GROUP * TOK
     lane = lax.broadcasted_iota(jnp.int32, (TOK, PAD), 1)
     key_pad = jnp.where(lane < 3, 1.0, 0.0).astype(F32)
@@ -84,7 +82,7 @@
         q_tok[at, :] = tok[:, :HEAD_DIM].astype(BF)
         g_tok[at, :] = tok[:, HEAD_DIM + PAD :].astype(BF)
         low, y = NEAR_ORDER[i]
-        k_block = k_all[y * 2 + (side[0] ^ low)]
+        k_block = k_all[low * 4 + y]
         k_t[:, at] = k_block[:HEAD_DIM]
         ktok = k_block.astype(F32).T
         k_tok[at, :] = jnp.concatenate([ktok[:, :HEAD_DIM], key_pad], axis=1).astype(BF)
@@ -150,12 +148,14 @@
     rot_grad[...] = around
 
 
-def call(body, args, outs, scratch=(), **more):
+def call(body, args, outs, name, scratch=(), **more):
     shapes = [
         pltpu.VMEM(shape, kind) if near else jax.ShapeDtypeStruct(shape, kind)
         for shape, kind, near in outs
     ]
-    return pl.pallas_call(body, out_shape=shapes, scratch_shapes=list(scratch), **more)(*args)
+    return pl.pallas_call(body, out_shape=shapes, scratch_shapes=list(scratch), name=name, **more)(
+        *args
+    )
 
 
 def close(x):
@@ -174,20 +174,25 @@
 
 def per_device(queries, latents, rot_key, kv_weight, log_sums, outputs, out_grad):
     total = GROUP * TOK
-    k_send, q_send, latents_kept = call(
-        prepare,
-        (latents, rot_key.T, kv_weight, queries.T, log_sums.T, outputs.T, out_grad.T),
-        [((K_ROWS, TOK), BF, True), ((GROUP, Q_ROWS, TOK), BF, False), (latents.shape, BF, True)],
-    )
-    k_other = lax.ppermute(k_send, "sp", [(i, i ^ 4) for i in range(64)])
+    (q_send,) = call(
+        prepare_queries,
+        (queries.T, log_sums.T, outputs.T, out_grad.T),
+        [((GROUP, Q_ROWS, TOK), BF, False)],
+        "prepare_queries",
+    )
+    k_send, latents_kept = call(
+        prepare_keys,
+        (latents, rot_key.T, kv_weight),
+        [((K_ROWS, TOK), BF, True), (latents.shape, BF, True)],
+        "prepare_keys",
+    )
     q_all = exchange(q_send, OUT)
-    (k_pair,) = call(pair, (close(k_send), close(k_other)), [((2, K_ROWS, TOK), BF, True)])
-    k_all = close(gather_pairs(k_pair, "sp", 64, (1, 2)).reshape(GROUP, K_ROWS, TOK))
-    side = (lax.axis_index("sp") // 4 % 2).astype(jnp.int32).reshape(1)
+    k_all = close(gather_pairs(k_send, "sp", 64, (1, 2, 4)).reshape(GROUP, K_ROWS, TOK))
     dq, dkv = call(
         attend,
-        (side, q_all, k_all),
+        (q_all, k_all),
         [((GROUP, HEAD_DIM, TOK), BF, True), ((GROUP, K_ROWS, TOK), BF, True)],
+        "attend",
         [
             pltpu.VMEM((Q_ROWS, total), BF),
             pltpu.VMEM((total, HEAD_DIM), BF),
@@ -201,7 +206,6 @@
             pltpu.VMEM((total, total), BF),
             pltpu.VMEM((total, total), BF),
         ],
-        in_specs=[pl.BlockSpec(memory_space=where) for where in (pltpu.SMEM, pltpu.VMEM, pltpu.VMEM)],
     )
     key_grad, value_grad, rot_send, weight_send = call(
         finish_keys,
@@ -212,25 +216,31 @@
             ((ROPE_DIM, TOK), F32, True),
             ((GROUP, GROUP * 8, TOK), BF, True),
         ],
-    )
-    rot_all = close(gather_pairs(rot_send, "tp", 8, (1, 2, 4)).reshape(GROUP, ROPE_DIM, TOK))
+        "finish_keys",
+    )
+    rot_all = close(gather_pairs(rot_send, "tp", 8, (4, 2, 1)).reshape(GROUP, ROPE_DIM, TOK))
     (far_send,) = call(
-        join_far, (exchange(weight_send, NEAR), close(dq)), [((GROUP, FAR_ROWS, TOK), BF, False)]
+        join_far,
+        (exchange(weight_send, NEAR), close(dq)),
+        [((GROUP, FAR_ROWS, TOK), BF, False)],
+        "join_far",
     )
     query_grad, weight_grad, rot_grad = call(
         finish_rest,
         (exchange(far_send, BACK), rot_all),
         [((HEAD_DIM, TOK), BF, False), ((8, TOK), F32, False), ((ROPE_DIM, TOK), F32, False)],
+        "finish_rest",
     )
     return query_grad.T, key_grad.T, value_grad.T, rot_grad.T, weight_grad
 
 
 def solution(mesh):
     placed = (P("sp", "tp"), P("sp", None), P("sp", None), P(None, "tp"), P("sp", "tp"), P("sp", "tp"), P("sp", "tp"))
-    return jax.shard_map(
+    step = jax.shard_map(
         per_device,
         mesh=mesh,
         in_specs=placed,
         out_specs=(P("sp", "tp"), P("sp", "tp"), P("sp", "tp"), P("sp", None), P("sp", "tp")),
         check_vma=False,
     )
+    return step

time: 93.6 us -> 84.5 us (0.903)
  waiting for transfers between devices: 13.6 us -> 0.82 us
  blocking collectives: 47 us -> 52 us
  starting transfers between devices: 24.7 us -> 22.6 us
    ppermute x1 -> x0, waiting for transfers between devices: 13.6 us -> none  [per_device(): k_other = lax.ppermute(k_send, 'sp', [(i, i ^ 4) for i in range(64)])]
    all_gather x5 -> x6, blocking collectives: 25.4 us -> 30.3 us  [gather_pairs(): x = lax.all_gather(x, axis, axis_index_groups=pairs(count, bit))]
    ppermute x1 -> x0, starting transfers between devices: 2.91 us -> none  [per_device(): k_other = lax.ppermute(k_send, 'sp', [(i, i ^ 4) for i in range(64)])]
  transfers between devices with their start and end apart: 3 -> 2, of which waited for: 1 -> 1; matrix products, arithmetic and copies ran while one was open for 0% -> 0% of each run, Pallas kernels for 0% -> 1%
where the time goes in v9:
time: 84.5 us; the launch traced here: 83.7 us
  blocking collectives  52 us (62%)
  starting transfers between devices  22.6 us (27%)
  Pallas kernels  7.66 us (9%)
    all_gather x6, blocking collectives, gather_pairs(): x = lax.all_gather(x, axis, axis_index_groups=pairs(count, bit))  30.3 us
    all_to_all x2, starting transfers between devices, exchange(): lax.all_to_all(x, 'sp', 0, 0, axis_index_groups=groups, tiled=True)  22.6 us
    all_to_all x2, blocking collectives, exchange(): lax.all_to_all(x, 'sp', 0, 0, axis_index_groups=groups, tiled=True)  21.7 us
    pallas_call x6, Pallas kernels, call(): pl.pallas_call(body, out_shape=shapes, scratch_shapes=list(scratch), name...  7.66 us
  transfers between devices with their start and end apart: 2, of which 1 were waited for; matrix products, arithmetic and copies ran while one was open for 0% of the time, Pallas kernels for 1%

profile of v9, /device:TPU:6, one launch (start us, length us, event | category | flops | bytes accessed | tf_op | source)
XLA Modules:
  0.0 83.7 jit_solution(12269994272083815299)
XLA Ops:
  0.6 1.5 %prepare_queries.1 = bf16[8,168,128]{2,1,0:T(8,128)(2,1)} custom-call(bf16[96,128]{1,0:T(8,128)(2,1)} %bitcast.21, f32[1,128]{1,0:T(1,128)} %bitcast.25, bf16[64,128]{1,0:T(8,128)(2,1)} %bitcast.22, bf16[64,128]{1,0:T(8,128)(2,1)} %bitcast.23), custom_call_target="tpu_custom_call" | custom-call | tf_op jit(solution)/shard_map/prepare_queries/pallas_call | solution.py:156
  2.2 18.4 %all-to-all-start = ((bf16[8,168,128]{2,1,0:T(8,128)(2,1)}), bf16[8,168,128]{2,1,0:T(8,128)(2,1)S(1)}, u32[]{:S(2)}, u32[]{:S(2)}) async-start(bf16[8,168,128]{2,1,0:T(8,128)(2,1)} %prepare_queries.1), calls=%async_computation | async-start | bytes 688128 | tf_op jit(solution)/shard_map/all_to_all | solution.py:166
  20.5 1.2 %prepare_keys.1 = (bf16[160,128]{1,0:T(8,128)(2,1)S(1)}, bf16[128,512]{1,0:T(8,128)(2,1)S(1)}) custom-call(bf16[128,512]{1,0:T(8,128)(2,1)} %latents.1, bf16[32,128]{1,0:T(8,128)(2,1)} %bitcast.24, bf16[512,128]{1,0:T(8,128)(2,1)} %weight.1), custom_call_target="tpu_custom_call" | custom-call | tf_op jit(solution)/shard_map/prepare_keys/pallas_call | solution.py:156
  21.8 4.7 %all-gather = bf16[320,128]{1,0:T(8,128)(2,1)S(1)} all-gather(bf16[160,128]{1,0:T(8,128)(2,1)S(1)} %get-tuple-element.16), channel_id=2, replica_groups={{0,8},{16,24},{32,40},{48,56},{64,72},{80,88},{96,104},{112,120},{128,1..., dimensions={0}, use_global_device_ids=true | all-gather | bytes 122880 | tf_op jit(solution)/shard_map/all_gather | solution.py:171
  26.5 6.6 %all-gather.1 = bf16[4,160,128]{2,1,0:T(8,128)(2,1)S(1)} all-gather(bf16[2,160,128]{2,1,0:T(8,128)(2,1)S(1)} %bitcast.18), channel_id=3, replica_groups={{0,16},{8,24},{32,48},{40,56},{64,80},{72,88},{96,112},{104,120},{128,1..., dimensions={0}, use_global_device_ids=true | all-gather | bytes 245760 | tf_op jit(solution)/shard_map/all_gather | solution.py:171
  33.1 6.7 %all-gather.2 = bf16[4,2,160,128]{3,2,1,0:T(8,128)(2,1)S(1)} all-gather(bf16[2,2,160,128]{3,2,1,0:T(8,128)(2,1)S(1)} %bitcast.17), channel_id=4, replica_groups={{0,32},{8,40},{16,48},{24,56},{64,96},{72,104},{80,112},{88,120},{128,1..., dimensions={0}, use_global_device_ids=true | all-gather | bytes 491520 | tf_op jit(solution)/shard_map/all_gather | solution.py:171
  39.7 0.0 all-to-all-done.q_all
  39.8 2.9 %attend.1 = (bf16[8,96,128]{2,1,0:T(8,128)(2,1)S(1)}, bf16[8,160,128]{2,1,0:T(8,128)(2,1)S(1)}) custom-call(bf16[8,168,128]{2,1,0:T(8,128)(2,1)S(1)} %all-to-all-done.q_all, bf16[8,160,128]{2,1,0:T(8,128)(2,1)S(1)} %bitcast.15), custom_call_target="tpu_custom_call" | custom-call | tf_op jit(solution)/shard_map/attend/pallas_call | solution.py:156
  42.7 12.5 %all_to_all.20.dkv = bf16[8,160,128]{2,1,0:T(8,128)(2,1)S(1)} all-to-all(bf16[8,160,128]{2,1,0:T(8,128)(2,1)S(1)} %get-tuple-element.17), channel_id=1, replica_groups={{0,32,16,48,8,40,24,56},{64,96,80,112,72,104,88,120},{128,160,144,176,1..., dimensions={0} | all-to-all | bytes 655360 | tf_op jit(solution)/shard_map/all_to_all | solution.py:166
  55.2 0.7 finish_keys.1
  55.8 9.1 %all_to_all.21.weight = bf16[8,64,128]{2,1,0:T(8,128)(2,1)S(1)} all-to-all(bf16[8,64,128]{2,1,0:T(8,128)(2,1)S(1)} %get-tuple-element.19), channel_id=1, replica_groups={{0,32,16,48,8,40,24,56},{64,96,80,112,72,104,88,120},{128,160,144,176,1..., dimensions={0} | all-to-all | bytes 262144 | tf_op jit(solution)/shard_map/all_to_all | solution.py:166
  65.0 0.7 join_far.1
  65.7 4.2 %all-to-all-start.3 = ((bf16[8,104,128]{2,1,0:T(8,128)(2,1)}), bf16[8,104,128]{2,1,0:T(8,128)(2,1)S(1)}, u32[]{:S(2)}, u32[]{:S(2)}) async-start(bf16[8,104,128]{2,1,0:T(8,128)(2,1)} %join_far.1), calls=%async_computation.3 | async-start | bytes 425984 | tf_op jit(solution)/shard_map/all_to_all | solution.py:166
  69.8 5.9 %all-gather.3 = f32[64,128]{1,0:T(8,128)S(1)} all-gather(f32[32,128]{1,0:T(8,128)S(1)} %get-tuple-element.21), channel_id=5, replica_groups={{0,4},{1,5},{2,6},{3,7},{8,12},{9,13},{10,14},{11,15},{16,20},{17,21},{..., dimensions={0}, use_global_device_ids=true | all-gather | bytes 49152 | tf_op jit(solution)/shard_map/all_gather | solution.py:171
  75.7 4.6 %all-gather.4 = f32[4,32,128]{2,1,0:T(8,128)S(1)} all-gather(f32[2,32,128]{2,1,0:T(8,128)S(1)} %bitcast.20), channel_id=6, replica_groups={{0,2},{1,3},{4,6},{5,7},{8,10},{9,11},{12,14},{13,15},{16,18},{17,19},{..., dimensions={0}, use_global_device_ids=true | all-gather | bytes 98304 | tf_op jit(solution)/shard_map/all_gather | solution.py:171
  80.3 1.9 %all-gather.5 = f32[4,2,32,128]{3,2,1,0:T(8,128)S(1)} all-gather(f32[2,2,32,128]{3,2,1,0:T(8,128)S(1)} %bitcast.19), channel_id=7, replica_groups={{0,1},{2,3},{4,5},{6,7},{8,9},{10,11},{12,13},{14,15},{16,17},{18,19},{..., dimensions={0}, use_global_device_ids=true | all-gather | bytes 196608 | tf_op jit(solution)/shard_map/all_gather | solution.py:171
  82.2 0.8 all-to-all-done.3.far
  83.0 0.6 finish_rest.1
Async XLA Ops:
  2.2 37.6 %all-to-all-start = ((bf16[8,168,128]{2,1,0:T(8,128)(2,1)}), bf16[8,168,128]{2,1,0:T(8,128)(2,1)S(1)}, u32[]{:S(2)}, u32[]{:S(2)}) async-start(bf16[8,168,128]{2,1,0:T(8,128)(2,1)} %prepare_queries.1), calls=%async_computation | async-start | bytes 688128 | tf_op jit(solution)/shard_map/all_to_all | solution.py:166
  65.7 17.4 %all-to-all-start.3 = ((bf16[8,104,128]{2,1,0:T(8,128)(2,1)}), bf16[8,104,128]{2,1,0:T(8,128)(2,1)S(1)}, u32[]{:S(2)}, u32[]{:S(2)}) async-start(bf16[8,104,128]{2,1,0:T(8,128)(2,1)} %join_far.1), calls=%async_computation.3 | async-start | bytes 425984 | tf_op jit(solution)/shard_map/all_to_all | solution.py:166

commit v10 on v9

--- a/solution.py
+++ b/solution.py
@@ -55,7 +55,7 @@
     k_out[HEAD_DIM:] = joined_t[NOPE_DIM:]
 
 
-def prepare_queries(queries, logs, outputs, grads, q_out):
+def prepare_queries(queries, logs, outputs, grads, q_out, block, sems):
     q_t = queries[...].astype(F32)
     g_t = grads[...].astype(F32)
     delta = jnp.sum(outputs[...].astype(F32) * g_t, axis=0, keepdims=True)
@@ -64,9 +64,12 @@
     pad = jnp.zeros((PAD, TOK), F32)
     for i, row in enumerate(rows):
         pad = jnp.where(index == i, row, pad)
-    block = jnp.concatenate([q_t, pad, g_t], axis=0).astype(BF)
-    for i in range(GROUP):
-        q_out[i] = block
+    block[...] = jnp.concatenate([q_t, pad, g_t], axis=0).astype(BF)
+    copies = [pltpu.make_async_copy(block, q_out.at[i], sems.at[i]) for i in range(GROUP)]
+    for copy in copies:
+        copy.start()
+    for copy in copies:
+        copy.wait()
 
 
 def attend(q_all, k_all, dq_out, dkv_out, q_t, q_tok, g_tok, k_t, k_tok, v_tok, dq_acc, dk_acc, dv_acc, dscores, probs_b):
@@ -179,6 +182,8 @@
         (queries.T, log_sums.T, outputs.T, out_grad.T),
         [((GROUP, Q_ROWS, TOK), BF, False)],
         "prepare_queries",
+        [pltpu.VMEM((Q_ROWS, TOK), BF), pltpu.SemaphoreType.DMA((GROUP,))],
+        out_specs=[pl.BlockSpec(memory_space=pl.ANY)],
     )
     k_send, latents_kept = call(
         prepare_keys,

time: 84.5 us -> 84.6 us (level)
  no operation moved by 1% of the time
where the time goes in v10:
time: 84.6 us; the launch traced here: 83.7 us
  blocking collectives  52 us (61%)
  starting transfers between devices  22.6 us (27%)
  Pallas kernels  7.72 us (9%)
    all_gather x6, blocking collectives, gather_pairs(): x = lax.all_gather(x, axis, axis_index_groups=pairs(count, bit))  30.3 us
    all_to_all x2, starting transfers between devices, exchange(): lax.all_to_all(x, 'sp', 0, 0, axis_index_groups=groups, tiled=True)  22.6 us
    all_to_all x2, blocking collectives, exchange(): lax.all_to_all(x, 'sp', 0, 0, axis_index_groups=groups, tiled=True)  21.6 us
    pallas_call x6, Pallas kernels, call(): pl.pallas_call(body, out_shape=shapes, scratch_shapes=list(scratch), name...  7.72 us
  transfers between devices with their start and end apart: 2, of which 1 were waited for; matrix products, arithmetic and copies ran while one was open for 0% of the time, Pallas kernels for 1%

profile of v10, /device:TPU:6, one launch (start us, length us, event | category | flops | bytes accessed | tf_op | source)
XLA Modules:
  0.0 83.7 jit_solution(6667611156564933898)
XLA Ops:
  0.6 1.6 %prepare_queries.1 = bf16[8,168,128]{2,1,0:T(8,128)(2,1)} custom-call(bf16[96,128]{1,0:T(8,128)(2,1)} %bitcast.21, f32[1,128]{1,0:T(1,128)} %bitcast.25, bf16[64,128]{1,0:T(8,128)(2,1)} %bitcast.22, bf16[64,128]{1,0:T(8,128)(2,1)} %bitcast.23), custom_call_target="tpu_custom_call" | custom-call | tf_op jit(solution)/shard_map/prepare_queries/pallas_call | solution.py:159
  2.2 18.4 %all-to-all-start = ((bf16[8,168,128]{2,1,0:T(8,128)(2,1)}), bf16[8,168,128]{2,1,0:T(8,128)(2,1)S(1)}, u32[]{:S(2)}, u32[]{:S(2)}) async-start(bf16[8,168,128]{2,1,0:T(8,128)(2,1)} %prepare_queries.1), calls=%async_computation | async-start | bytes 688128 | tf_op jit(solution)/shard_map/all_to_all | solution.py:169
  20.6 1.2 %prepare_keys.1 = (bf16[160,128]{1,0:T(8,128)(2,1)S(1)}, bf16[128,512]{1,0:T(8,128)(2,1)S(1)}) custom-call(bf16[128,512]{1,0:T(8,128)(2,1)} %latents.1, bf16[32,128]{1,0:T(8,128)(2,1)} %bitcast.24, bf16[512,128]{1,0:T(8,128)(2,1)} %weight.1), custom_call_target="tpu_custom_call" | custom-call | tf_op jit(solution)/shard_map/prepare_keys/pallas_call | solution.py:159
  21.9 4.7 %all-gather = bf16[320,128]{1,0:T(8,128)(2,1)S(1)} all-gather(bf16[160,128]{1,0:T(8,128)(2,1)S(1)} %get-tuple-element.16), channel_id=2, replica_groups={{0,8},{16,24},{32,40},{48,56},{64,72},{80,88},{96,104},{112,120},{128,1..., dimensions={0}, use_global_device_ids=true | all-gather | bytes 122880 | tf_op jit(solution)/shard_map/all_gather | solution.py:174
  26.5 6.6 %all-gather.1 = bf16[4,160,128]{2,1,0:T(8,128)(2,1)S(1)} all-gather(bf16[2,160,128]{2,1,0:T(8,128)(2,1)S(1)} %bitcast.18), channel_id=3, replica_groups={{0,16},{8,24},{32,48},{40,56},{64,80},{72,88},{96,112},{104,120},{128,1..., dimensions={0}, use_global_device_ids=true | all-gather | bytes 245760 | tf_op jit(solution)/shard_map/all_gather | solution.py:174
  33.1 6.7 %all-gather.2 = bf16[4,2,160,128]{3,2,1,0:T(8,128)(2,1)S(1)} all-gather(bf16[2,2,160,128]{3,2,1,0:T(8,128)(2,1)S(1)} %bitcast.17), channel_id=4, replica_groups={{0,32},{8,40},{16,48},{24,56},{64,96},{72,104},{80,112},{88,120},{128,1..., dimensions={0}, use_global_device_ids=true | all-gather | bytes 491520 | tf_op jit(solution)/shard_map/all_gather | solution.py:174
  39.8 0.0 all-to-all-done.q_all
  39.8 2.9 %attend.1 = (bf16[8,96,128]{2,1,0:T(8,128)(2,1)S(1)}, bf16[8,160,128]{2,1,0:T(8,128)(2,1)S(1)}) custom-call(bf16[8,168,128]{2,1,0:T(8,128)(2,1)S(1)} %all-to-all-done.q_all, bf16[8,160,128]{2,1,0:T(8,128)(2,1)S(1)} %bitcast.15), custom_call_target="tpu_custom_call" | custom-call | tf_op jit(solution)/shard_map/attend/pallas_call | solution.py:159
  42.7 12.5 %all_to_all.20.dkv = bf16[8,160,128]{2,1,0:T(8,128)(2,1)S(1)} all-to-all(bf16[8,160,128]{2,1,0:T(8,128)(2,1)S(1)} %get-tuple-element.17), channel_id=1, replica_groups={{0,32,16,48,8,40,24,56},{64,96,80,112,72,104,88,120},{128,160,144,176,1..., dimensions={0} | all-to-all | bytes 655360 | tf_op jit(solution)/shard_map/all_to_all | solution.py:169
  55.2 0.7 finish_keys.1
  55.9 9.1 %all_to_all.21.weight = bf16[8,64,128]{2,1,0:T(8,128)(2,1)S(1)} all-to-all(bf16[8,64,128]{2,1,0:T(8,128)(2,1)S(1)} %get-tuple-element.19), channel_id=1, replica_groups={{0,32,16,48,8,40,24,56},{64,96,80,112,72,104,88,120},{128,160,144,176,1..., dimensions={0} | all-to-all | bytes 262144 | tf_op jit(solution)/shard_map/all_to_all | solution.py:169
  65.0 0.7 join_far.1
  65.7 4.2 %all-to-all-start.3 = ((bf16[8,104,128]{2,1,0:T(8,128)(2,1)}), bf16[8,104,128]{2,1,0:T(8,128)(2,1)S(1)}, u32[]{:S(2)}, u32[]{:S(2)}) async-start(bf16[8,104,128]{2,1,0:T(8,128)(2,1)} %join_far.1), calls=%async_computation.3 | async-start | bytes 425984 | tf_op jit(solution)/shard_map/all_to_all | solution.py:169
  69.9 5.9 %all-gather.3 = f32[64,128]{1,0:T(8,128)S(1)} all-gather(f32[32,128]{1,0:T(8,128)S(1)} %get-tuple-element.21), channel_id=5, replica_groups={{0,4},{1,5},{2,6},{3,7},{8,12},{9,13},{10,14},{11,15},{16,20},{17,21},{..., dimensions={0}, use_global_device_ids=true | all-gather | bytes 49152 | tf_op jit(solution)/shard_map/all_gather | solution.py:174
  75.8 4.6 %all-gather.4 = f32[4,32,128]{2,1,0:T(8,128)S(1)} all-gather(f32[2,32,128]{2,1,0:T(8,128)S(1)} %bitcast.20), channel_id=6, replica_groups={{0,2},{1,3},{4,6},{5,7},{8,10},{9,11},{12,14},{13,15},{16,18},{17,19},{..., dimensions={0}, use_global_device_ids=true | all-gather | bytes 98304 | tf_op jit(solution)/shard_map/all_gather | solution.py:174
  80.4 1.9 %all-gather.5 = f32[4,2,32,128]{3,2,1,0:T(8,128)S(1)} all-gather(f32[2,2,32,128]{3,2,1,0:T(8,128)S(1)} %bitcast.19), channel_id=7, replica_groups={{0,1},{2,3},{4,5},{6,7},{8,9},{10,11},{12,13},{14,15},{16,17},{18,19},{..., dimensions={0}, use_global_device_ids=true | all-gather | bytes 196608 | tf_op jit(solution)/shard_map/all_gather | solution.py:174
  82.3 0.8 all-to-all-done.3.far
  83.1 0.6 finish_rest.1
Async XLA Ops:
  2.2 37.6 %all-to-all-start = ((bf16[8,168,128]{2,1,0:T(8,128)(2,1)}), bf16[8,168,128]{2,1,0:T(8,128)(2,1)S(1)}, u32[]{:S(2)}, u32[]{:S(2)}) async-start(bf16[8,168,128]{2,1,0:T(8,128)(2,1)} %prepare_queries.1), calls=%async_computation | async-start | bytes 688128 | tf_op jit(solution)/shard_map/all_to_all | solution.py:169
  65.7 17.4 %all-to-all-start.3 = ((bf16[8,104,128]{2,1,0:T(8,128)(2,1)}), bf16[8,104,128]{2,1,0:T(8,128)(2,1)S(1)}, u32[]{:S(2)}, u32[]{:S(2)}) async-start(bf16[8,104,128]{2,1,0:T(8,128)(2,1)} %join_far.1), calls=%async_computation.3 | async-start | bytes 425984 | tf_op jit(solution)/shard_map/all_to_all | solution.py:169
